TPU v7x, 32 devices: a whole 2x2x4 slice. The times are simulated.
32 devices in a mesh: sp: 8 (over z, x), tp: 4 (over y, core).
Axes of the slice: x: 2, y: 2, z: 4, core: 2. Of those that a mesh axis runs over, the one named last changes fastest.
Arguments:
- tokens: bfloat16 [3072, 2048], P(('sp', 'tp')), may hold values from -6 to 6
- norm_gain: float32 [2048], replicated, may hold values from 0.1 to 1.9
- w_recept: bfloat16 [2048, 1024], P(None, 'tp'), may hold values from -0.125 to 0.125
- w_key: bfloat16 [2048, 1024], P(None, 'tp'), may hold values from -0.125 to 0.125
- w_value: bfloat16 [2048, 1024], P(None, 'tp'), may hold values from -0.125 to 0.125
- w_decay: bfloat16 [2048, 1024], P(None, 'tp'), may hold values from -0.125 to 0.125
- w_rate: bfloat16 [2048, 1024], P(None, 'tp'), may hold values from -0.125 to 0.125
- w_gate: bfloat16 [2048, 1024], P(None, 'tp'), may hold values from -0.125 to 0.125
- shift_mix: float32 [3, 1024], P(None, 'tp'), may hold values from 0 to 1
- decay_base: float32 [1024], P('tp'), may hold values from -16 to -2
- rate_base: float32 [1024], P('tp'), may hold values from -10 to 1
- decay_drift: float32 [3072], P('sp'), may hold values from -2 to 2, as said below
- group_gain: float32 [1024], P('tp'), may hold values from 0.1 to 1.9
- initial_state: float32 [16, 64, 64], P('tp'), may hold values from -240 to 240
- w_out: bfloat16 [1024, 2048], replicated, may hold values from -0.1875 to 0.1875
Outputs:
- out: bfloat16 [3072, 2048], P(('sp', 'tp'))
Inputs may be any that keep to these rules, and one draw needn't show every extreme that they name: `decay_drift`: constant over aligned runs of 64 positions.
All inputs are finite; a program needn't handle non-finite values.
Results may differ from a plain program's by a relative error of at most 0.0083.
Values may be sent and summed in bfloat16 or wider, within the bound.
A program may use at most 128 MiB of HBM per device.

v0:
```python
import jax
import jax.numpy as jnp
from jax import lax
from jax.sharding import PartitionSpec as P

HEAD = 64
BLOCK = 64


norm_floor = 0.5
group_floor = 1.0
highest = lax.Precision.HIGHEST


def shifted_2(block, axis, distance):
    devices = range(lax.axis_size(axis))
    route = [(i - distance, i) for i in devices if i - distance in devices]
    return lax.ppermute(block, axis, route)


def carried_in(value, axis, join, neutral):
    count, mine = (lax.axis_size(axis), lax.axis_index(axis))
    pieces = jax.tree.map(lambda part: lax.all_gather(part, axis), value)
    running = jax.tree.map(
        lambda part, zero: jnp.full_like(part, 0) + jnp.asarray(zero, part.dtype), value, neutral
    )

    def turn(position, running):
        longer = join(running, jax.tree.map(lambda part: part[position], pieces))
        return jax.tree.map(lambda new, old: jnp.where(position < mine, new, old), longer, running)

    return lax.fori_loop(0, count - 1, turn, running)


def block_masks(width):
    places = lax.broadcasted_iota(jnp.int32, (width, width), 0)
    others = lax.broadcasted_iota(jnp.int32, (width, width), 1)
    return (others < places, others <= places)


def pair_dots(left, right):
    return jnp.einsum("bhtn,bhsn->bhts", left, right, precision=highest)


def chain_product(first, second):
    return jnp.einsum("hij,hjk->hik", first, second, precision=highest)


def prepare_blocks(streams):
    recept, decay, key, value, unit, rate = streams
    width = recept.shape[2]
    size = recept.shape[3]
    strict, inclusive = block_masks(width)
    logs = jnp.log(decay)
    running = jnp.cumsum(logs, axis=2)
    through = jnp.exp(running)
    until = jnp.exp(running - logs)
    alpha = -unit * until
    beta = unit * rate / through
    key_scaled = key / through
    recept_scaled = recept * through
    lower_ab = jnp.where(strict, pair_dots(alpha, beta), 0.0)
    lower_ak = jnp.where(strict, pair_dots(alpha, key_scaled), 0.0)
    system = jnp.eye(width, dtype=jnp.float32) - lower_ab
    targets = jnp.concatenate(
        [alpha, jnp.einsum("bhts,bhsr->bhtr", lower_ak, value, precision=highest)], axis=3
    )
    solved = jax.scipy.linalg.solve_triangular(system, targets, lower=True, unit_diagonal=True)
    solved_alpha = solved[..., :size]
    solved_value = solved[..., size:]
    final = through[:, :, -1:, :]
    beta_final = beta * final
    key_final = key_scaled * final
    transition = jnp.eye(size, dtype=jnp.float32) * final + jnp.einsum(
        "bhtm,bhtn->bhmn", solved_alpha, beta_final, precision=highest
    )
    added = jnp.einsum("bhtr,bhtn->bhrn", solved_value, beta_final, precision=highest) + jnp.einsum(
        "bhtr,bhtn->bhrn", value, key_final, precision=highest
    )
    upper_b = jnp.where(inclusive, pair_dots(recept_scaled, beta), 0.0)
    upper_k = jnp.where(inclusive, pair_dots(recept_scaled, key_scaled), 0.0)
    reads = recept_scaled + jnp.einsum("bhts,bhsn->bhtn", upper_b, solved_alpha, precision=highest)
    fixed_out = jnp.einsum(
        "bhts,bhsr->bhtr", upper_b, solved_value, precision=highest
    ) + jnp.einsum("bhts,bhsr->bhtr", upper_k, value, precision=highest)
    return (transition, added, reads, fixed_out)


def run_blocks(start, prepared, extra_rows):
    transition, added, reads, fixed_out = prepared
    added = jnp.concatenate(
        [added, jnp.zeros(added.shape[:2] + (extra_rows, added.shape[3]), jnp.float32)], axis=2
    )
    fixed_out = jnp.concatenate(
        [fixed_out, jnp.zeros(fixed_out.shape[:3] + (extra_rows,), jnp.float32)], axis=3
    )

    def block_step(state, inputs):
        trans_now, added_now, reads_now, fixed_now = inputs
        new_state = jnp.einsum("hrm,hmn->hrn", state, trans_now, precision=highest) + added_now
        readout = jnp.einsum("htn,hrn->htr", reads_now, state, precision=highest) + fixed_now
        return (new_state, readout)

    return lax.scan(block_step, start, (transition, added, reads, fixed_out))


def per_device(
    tokens,
    norm_gain,
    w_recept,
    w_key,
    w_value,
    w_decay,
    w_rate,
    w_gate,
    shift_mix,
    decay_base,
    rate_base,
    decay_drift,
    group_gain,
    initial_state,
    w_out,
):
    tok_float = tokens.astype(jnp.float32)
    normed = (
        tok_float
        * lax.rsqrt(jnp.mean(tok_float * tok_float, axis=-1, keepdims=True) + norm_floor)
        * norm_gain
    ).astype(jnp.bfloat16)
    weights = (w_recept, w_key, w_value, w_decay, w_rate, w_gate)
    piece = lax.all_gather(normed, "tp", axis=0, tiled=True)
    projected = jnp.stack(
        [
            jnp.dot(piece, weight, preferred_element_type=jnp.float32).astype(jnp.bfloat16)
            for weight in weights
        ],
        axis=0,
    )
    edge_rows = projected[0:3, -1:, :]
    earlier_rows = shifted_2(edge_rows, "sp", 1)
    current = projected[0:3].astype(jnp.float32)
    earlier = jnp.concatenate([earlier_rows.astype(jnp.float32), current[:, :-1]], axis=1)
    shifted = current + (earlier - current) * shift_mix[:, None, :]
    recept, key, value = (shifted[0], shifted[1], shifted[2])
    level = decay_base + projected[3].astype(jnp.float32) + decay_drift[:, None]
    decay = jnp.exp(-jnp.exp(-jax.nn.softplus(-level) - 0.5))
    rate = jax.nn.sigmoid(rate_base + projected[4].astype(jnp.float32))
    gate = jax.nn.sigmoid(projected[5].astype(jnp.float32))
    seq_rows, local_width = recept.shape
    local_heads = local_width // HEAD
    block_count = seq_rows // BLOCK

    def blocked(array):
        return array.reshape(block_count, BLOCK, local_heads, HEAD).transpose(0, 2, 1, 3)

    key_heads = key.reshape(seq_rows, local_heads, HEAD)
    unit = key_heads * lax.rsqrt(jnp.sum(key_heads * key_heads, axis=-1, keepdims=True) + 1.0)
    streams = (
        blocked(recept),
        blocked(decay),
        blocked(key),
        blocked(value),
        blocked(unit.reshape(seq_rows, local_width)),
        blocked(rate),
    )
    prepared = prepare_blocks(streams)
    identity = jnp.broadcast_to(jnp.eye(HEAD, dtype=jnp.float32), (local_heads, HEAD, HEAD))
    empty = jnp.zeros((local_heads, HEAD, HEAD), jnp.float32)
    start_state = jnp.concatenate([empty, identity], axis=1)

    def combine(earlier_pair, later_pair):
        first_map, first_add = earlier_pair
        second_map, second_add = later_pair
        return (
            chain_product(first_map, second_map),
            chain_product(first_add, second_map) + second_add,
        )

    stretch, readout = run_blocks(start_state, prepared, HEAD)
    prefix_map, prefix_add = carried_in(
        (stretch[:, HEAD:], stretch[:, :HEAD]), "sp", combine, (identity, empty)
    )
    carried = chain_product(initial_state, prefix_map) + prefix_add
    mixed = readout[..., :HEAD] + jnp.einsum(
        "bhtj,hvj->bhtv", readout[..., HEAD:], carried, precision=highest
    )
    center = mixed - jnp.mean(mixed, axis=-1, keepdims=True)
    spread = jnp.mean(center * center, axis=-1, keepdims=True)
    gains = group_gain.reshape(local_heads, HEAD)[None, :, None, :]
    scaled = center * lax.rsqrt(spread + group_floor) * gains
    flat = scaled.transpose(0, 2, 1, 3).reshape(seq_rows, local_width)
    gated = (flat * gate).astype(jnp.bfloat16)
    token_rows = lax.all_to_all(gated, "tp", split_axis=0, concat_axis=1, tiled=True)
    result = jnp.dot(token_rows, w_out, preferred_element_type=jnp.float32).astype(jnp.bfloat16)
    return result


def solution(mesh):
    return jax.shard_map(
        per_device,
        mesh=mesh,
        in_specs=(
            P(("sp", "tp"), None),
            P(),
            P(None, "tp"),
            P(None, "tp"),
            P(None, "tp"),
            P(None, "tp"),
            P(None, "tp"),
            P(None, "tp"),
            P(None, "tp"),
            P("tp"),
            P("tp"),
            P("sp"),
            P("tp"),
            P("tp", None, None),
            P(),
        ),
        out_specs=P(("sp", "tp"), None),
        check_vma=False,
    )
```

profile of v0, /device:TPU:27, one launch (start us, length us, event | category | flops | bytes accessed | tf_op | source)
XLA Modules:
  0.0 322.5 jit_solution(3846499401676920296)
XLA Ops:
  6.5 1.3 fusion.51
  7.8 1.9 fusion.53
  9.9 0.6 fusion.85
  11.2 0.8 concatenate.17
  11.9 0.6 iota_compare_fusion
  12.5 0.7 iota_compare_fusion.2
  13.2 17.7 %all-gather.4.cloned.1.call-done = bf16[384,2048]{1,0:T(8,128)(2,1)} async-done(((bf16[96,2048]{1,0:T(8,128)(2,1)}), bf16[384,2048]{1,0:T(8,128)(2,1)}) %all-gather.4.cloned.1.call-update) | async-done | bytes 1572880 | tf_op jit(solution)/shard_map/all_gather | solution.py:131
  30.9 2.1 fusion.48
  33.6 0.6 copy-done.27
  35.1 1.4 collective-permute-start
  36.5 1.6 fusion.81
  38.7 1.3 reshape.65
  40.0 1.3 log.10
  41.3 1.1 copy.125
  42.5 1.8 reduce_window_sum.11
  44.3 1.2 fusion.28
  45.5 1.1 fusion.89
  46.9 1.3 reshape_squeeze.10
  48.2 2.0 bitcast_divide_fusion.1
  50.3 2.4 convolution_select_fusion.2
  52.8 1.4 fusion.26
  54.2 118.6 %custom-call.4 = f32[6,4,1,64,64]{3,4,2,1,0:T(8,128)} custom-call(f32[6,4,1,64,64]{4,3,2,1,0:T(8,128)S(1)} %fusion.26), custom_call_target="InvertDiagBlocksLowerTriangular" | custom-call | tf_op jit(solution)/shard_map/jit(_solve_triangular)/vmap(vmap())/triangular_solve | solution.py:68
  172.8 1.3 reshape_squeeze.11
  174.1 0.9 copy-done.1
  175.0 2.2 fusion.61
  177.2 1.6 fusion.55
  178.9 2.3 convolution_add_fusion.4
  181.2 2.6 fusion.67
  183.7 2.2 reshape_squeeze.12
  186.0 2.7 convolution_select_fusion.1
  188.7 1.5 convolution_select_fusion
  190.2 1.9 convolution_add_fusion.2
  192.1 1.0 fusion.65
  193.5 1.7 convolution_add_fusion.3
  195.2 0.9 convolution_add_fusion.1
  196.3 0.7 copy-done.9
  197.0 18.9 %while.28 = (s32[]{:T(128)}, f32[4,128,64]{1,2,0:T(8,128)S(1)}, f32[6,4,64,128]{3,2,1,0:T(8,128)}, f32[6,4,64,64]{3,2,1,0:T(8,128)}, f32[6,4,128,64]{2,3,1,0:T(8...) while((s32[]{:T(128)}, f32[4,128,64]{1,2,0:T(8,128)S(1)}, ...), condition=%wide.region_4.5_spmd, body=%wide.region_3.4_spmd.sunk | while | flops 50397184 | bytes 1312861 | solution.py:104
  197.0 1.8 fusion.138
  198.9 1.3 fusion.137
  200.2 1.8 fusion.138
  202.0 1.3 fusion.137
  203.3 1.8 fusion.138
  205.2 1.3 fusion.137
  206.5 1.8 fusion.138
  208.3 1.3 fusion.137
  209.6 1.8 fusion.138
  211.4 1.3 fusion.137
  212.8 1.8 fusion.138
  214.6 1.3 fusion.137
  216.1 29.7 %all-gather.1 = f32[32,64,64]{2,1,0:T(8,128)} all-gather(f32[4,64,64]{2,1,0:T(8,128)S(1)} %get-tuple-element.240), channel_id=3, replica_groups=mesh['sp'=8,'tp'=4] {'sp'}, dimensions={0}, use_global_device_ids=true | all-gather | bytes 589824 | tf_op jit(solution)/shard_map/all_gather | solution.py:23
  245.8 27.4 %all-gather = f32[32,64,64]{2,1,0:T(8,128)S(1)} all-gather(f32[4,64,64]{2,1,0:T(8,128)S(1)} %get-tuple-element.241), channel_id=2, replica_groups=mesh['sp'=8,'tp'=4] {'sp'}, dimensions={0}, use_global_device_ids=true | all-gather | bytes 589824 | tf_op jit(solution)/shard_map/all_gather | solution.py:23
  273.2 13.2 %while.29 = (s32[]{:T(128)}, f32[4,64,64]{1,2,0:T(8,128)S(1)}, f32[4,64,64]{1,2,0:T(8,128)S(1)}, s32[]{:T(128)}, f32[8,4,64,64]{3,2,1,0:T(8,128)S(1)}, /*index=5*/f32[8,4,64,64]{3,2,1,0:T(8,128)}, s32[]{:T(128)}, s32[]{:T(128)}) while((s32[]{:T(128)}, f32[4,64,64]{1,2,0:T(8,128)S(1)}, f32[4,64,64]{1,2,0:T(8,128)S(1)}, s32[]{:T(128)}, ...), condition=%wide.region_6.7_spmd.clone, body=%wide.region_5.6_spmd.clone.sunk | while | flops 25247748 | bytes 1575032 | solution.py:32
  273.6 0.9 constant_dynamic-slice_fusion.2
  275.5 0.9 constant_dynamic-slice_fusion.2
  277.4 0.9 constant_dynamic-slice_fusion.2
  279.3 0.9 constant_dynamic-slice_fusion.2
  281.2 0.9 constant_dynamic-slice_fusion.2
  283.1 0.9 constant_dynamic-slice_fusion.2
  285.0 0.9 constant_dynamic-slice_fusion.2
  286.4 1.6 copy.66
  288.4 3.7 %fusion.91 = (f32[6,4,64]{2,0,1:T(8,128)S(1)}, f32[6,4,64,64]{2,3,0,1:T(8,128)S(1)}) fusion(f32[4,64,64,1]{1,2,3,0:T(8,128)S(1)} %fusion.50, f32[6,4,64,128]{2,3,0,1:T(8,128)S(1)} %copy.66, f32[6,4,64,128]{3,2,1,0:T(8,128)} %get-tuple-element.153), kind=kOutput, calls=%fused_computation.138 | convolution fusion | flops 75692544 | bytes 1644544 | tf_op jit(solution)/shard_map/bhtj,hvj->bhtv/dot_general | solution.py:184
  293.2 2.4 fusion.35
  295.7 18.4 %all_to_all.19 = bf16[4,96,256]{2,1,0:T(8,128)(2,1)S(1)} all-to-all(bf16[4,96,256]{2,1,0:T(8,128)(2,1)S(1)} %bitcast.170), channel_id=1, replica_groups=mesh['sp'=8,'tp'=4] {'tp'}, dimensions={0} | all-to-all | bytes 393216 | tf_op jit(solution)/shard_map/all_to_all | solution.py:193
  314.1 1.6 convolution_convert_fusion
  (138 shorter events, 11.7 us)
Async XLA Ops:
  6.5 24.4 %copy-start = (bf16[2048,256]{1,0:T(8,128)(2,1)S(1)}, bf16[2048,256]{1,0:T(8,128)(2,1)}, u32[]{:S(2)}) copy-start(bf16[2048,256]{1,0:T(8,128)(2,1)} %param.23) | copy-start | bytes 3145732
  6.5 3.3 %copy-start.24 = (f32[256]{0:T(256)S(1)}, f32[256]{0:T(256)}, u32[]{:S(2)}) copy-start(f32[256]{0:T(256)} %param.31) | copy-start | bytes 3076
  6.5 24.4 %all-gather.4.cloned.1.call-start = ((), (), s32[]{:S(2)}) async-start(), calls=%async_computation.1 | async-start | bytes 1966080 | tf_op jit(solution)/shard_map/all_gather | solution.py:131
  10.5 0.6 copy-start.15
  13.2 19.8 %copy-start.26 = (bf16[2048,256]{1,0:T(8,128)(2,1)S(1)}, bf16[2048,256]{1,0:T(8,128)(2,1)}, u32[]{:S(2)}) copy-start(bf16[2048,256]{1,0:T(8,128)(2,1)} %param.22) | copy-start | bytes 3145732
  30.9 2.1 copy-start.25
  33.0 1.2 copy-start.27
  34.8 3.3 %copy-start.13 = (bf16[1,384,256]{2,1,0:T(8,128)(2,1)}, bf16[1,384,256]{2,1,0:T(8,128)(2,1)S(1)}, u32[]{:S(2)}) copy-start(bf16[1,384,256]{2,1,0:T(8,128)(2,1)S(1)} %fusion.46) | copy-start | bytes 589828
  34.8 1.6 copy-start.28
  34.9 1.6 copy-start.30
  34.9 1.6 copy-start.31
  35.0 3.1 copy-start.29
  35.0 3.1 copy-start.32
  35.1 9.2 %collective-permute-start = (bf16[3,1,256]{2,1,0:T(2,128)(2,1)S(1)}, bf16[3,1,256]{2,1,0:T(2,128)(2,1)S(1)}, u32[]{:S(2)}, u32[]{:S(2)}) collective-permute-start(bf16[3,1,256]{2,1,0:T(2,128)(2,1)S(1)} %slice.58), channel_id=1, source_target_pairs={{0,4},{4,8},{8,12},{12,16},{16,20},{20,24},{24,28},{1,5},{5,9},{9,... | collective-permute-start | bytes 4616 | tf_op jit(solution)/shard_map/ppermute | solution.py:18
  41.3 1.1 copy-start.5
  41.3 3.0 copy-start.23
  48.2 2.1 copy-start.3
  48.2 2.1 copy-start.21
  50.2 2.5 copy-start.6
  50.3 2.5 copy-start.16
  50.3 2.4 copy-start.18
  50.3 2.4 copy-start.22
  174.1 0.9 copy-start.1
  175.0 2.2 copy-start.7
  175.0 2.2 copy-start.14
  177.2 1.6 copy-start.17
  186.0 2.7 copy-start.4
  186.0 2.7 copy-start.8
  186.0 2.7 copy-start.20
  192.1 1.1 copy-start.2
  192.1 1.4 copy-start.12
  196.1 0.9 copy-start.9
  215.9 57.3 %copy-start.10 = (f32[4,64,64]{1,2,0:T(8,128)S(1)}, f32[4,64,64]{1,2,0:T(8,128)}, u32[]{:S(2)}) copy-start(f32[4,64,64]{1,2,0:T(8,128)} %custom-call.5) | copy-start | bytes 196612
  286.4 1.7 copy-start.19
  293.2 20.9 %copy-start.11 = (bf16[1024,2048]{1,0:T(8,128)(2,1)S(1)}, bf16[1024,2048]{1,0:T(8,128)(2,1)}, u32[]{:S(2)}) copy-start(bf16[1024,2048]{1,0:T(8,128)(2,1)} %param.33) | copy-start | bytes 12582916
Sparse Core Ops, SparseCore 0:
  9.9 20.9 all-gather.3
where the time goes:
time: 327 us; the launch traced here: 323 us
  other arithmetic  130 us (40%)
  blocking collectives  75.5 us (23%)
  matrix products  59.8 us (18%)
  local copies, waits for them, and re-layouts  23.2 us (7%)
  waiting for transfers between devices  17.7 us (5%)
  between operations  14 us (4%)
    another operation x2, other arithmetic, prepare_blocks(): jax.scipy.linalg.solve_triangular(system, targets, lower=True, unit_diago...  119 us
    all_gather x2, blocking collectives, carried_in(): pieces = jax.tree.map(lambda part: lax.all_gather(part, axis), value)  57.1 us
    all_to_all x1, blocking collectives, per_device(): lax.all_to_all(gated, 'tp', split_axis=0, concat_axis=1, tiled=True)  18.4 us
    all_gather x1, waiting for transfers between devices, per_device(): piece = lax.all_gather(normed, 'tp', axis=0, tiled=True)  17.7 us
    dot_general x6, matrix products, block_step(): jnp.einsum('htn,hrn->htr', reads_now, state, precision=highest) + fixed_now  10.9 us
    dot_general x4, matrix products, pair_dots(): return jnp.einsum('bhtn,bhsn->bhts', left, right, precision=highest)  8.01 us
    dot_general x6, matrix products, per_device(): jnp.dot(piece, weight, preferred_element_type=jnp.float32)  7.88 us
    dot_general x6, matrix products, block_step(): jnp.einsum('hrm,hmn->hrn', state, trans_now, precision=highest) + added_now  7.73 us
  transfers between devices with their start and end apart: 2, of which 1 were waited for; matrix products, arithmetic and copies ran while one was open for 3% of the time, Pallas kernels for 0%

commit v1 on v0

v1 whole, which is shorter than its diff:
```python
import functools

import jax
import jax.numpy as jnp
from jax import lax
from jax.experimental import pallas as pl
from jax.experimental.pallas import tpu as pltpu
from jax.sharding import PartitionSpec as P

HEAD = 64
BLOCK = 64
F32 = jnp.float32
BF16 = jnp.bfloat16

norm_floor = 0.5
group_floor = 1.0

NN = (((1,), (0,)), ((), ()))
NT = (((1,), (1,)), ((), ()))
TN = (((0,), (0,)), ((), ()))


def dot1(a, b, dims):
    return lax.dot_general(a, b, dims, preferred_element_type=F32)


def split(a):
    high = a.astype(BF16)
    return high, (a - high.astype(F32)).astype(BF16)


def mm(a, b, dims=NN):
    ah, al = split(a)
    bh, bl = split(b)
    return dot1(ah, bh, dims) + (dot1(ah, bl, dims) + dot1(al, bh, dims))


def sum_rows(a, ones):
    high, rest = split(a)
    mid, low = split(a - high.astype(F32))
    return dot1(ones, high, NN) + (dot1(ones, mid, NN) + dot1(ones, low, NN))


def scan_kernel(
    n,
    m,
    heads,
    blocks,
    drift_ref,
    proj_ref,
    edge_ref,
    mix_ref,
    dbase_ref,
    rbase_ref,
    gain_ref,
    init_ref,
    wout_ref,
    out_ref,
    last_row,
    reads,
    prefix,
    running,
    window,
    g_buf,
    r_buf,
    flat,
    gated,
    act,
    wout,
    w_sem,
    g_send,
    g_recv,
    a_send,
    a_recv,
):
    s = lax.axis_index("sp")
    t = lax.axis_index("tp")
    steps = []
    while (1 << len(steps)) < n:
        steps.append(1 << len(steps))

    barrier = pltpu.get_barrier_semaphore()
    for d in steps:
        for other, ok in ((s + d, s + d < n), (s - d, s - d >= 0)):

            @pl.when(ok)
            def _():
                pl.semaphore_signal(
                    barrier, inc=1, device_id={"sp": other, "tp": t}, device_id_type=pl.DeviceIdType.MESH
                )

    for q in range(1, m):
        pl.semaphore_signal(
            barrier, inc=1, device_id={"sp": s, "tp": lax.rem(t + q, m)}, device_id_type=pl.DeviceIdType.MESH
        )

    load = pltpu.make_async_copy(wout_ref, wout, w_sem)
    load.start()

    width = BLOCK
    rows_i = lax.broadcasted_iota(jnp.int32, (width, width), 0)
    cols_i = lax.broadcasted_iota(jnp.int32, (width, width), 1)
    strict = cols_i < rows_i
    incl = cols_i <= rows_i
    eye = jnp.where(cols_i == rows_i, 1.0, 0.0).astype(F32)
    ones = jnp.where(incl, 1.0, 0.0).astype(BF16)
    zeros = jnp.zeros((width, HEAD), F32)
    levels = []
    size = 1
    while size < width:
        same = (rows_i // (2 * size)) == (cols_i // (2 * size))
        levels.append(same & ((rows_i // size) % 2 == 1) & ((cols_i // size) % 2 == 0))
        size *= 2
    first_row = lax.broadcasted_iota(jnp.int32, (width, heads * HEAD), 0) == 0
    mix = mix_ref[...]
    dbase = dbase_ref[...].reshape(1, heads * HEAD)
    rbase = rbase_ref[...].reshape(1, heads * HEAD)
    gain = gain_ref[...].reshape(1, heads * HEAD)

    for j in range(3):
        last_row[j] = jnp.broadcast_to(edge_ref[j].astype(F32), (8, heads * HEAD))
    for h in range(heads):
        running[h] = jnp.concatenate([eye, zeros], axis=1)

    @pl.loop(0, blocks)
    def _(b):
        at = pl.ds(pl.multiple_of(b * width, width), width)

        def shifted(j):
            cur = proj_ref[j, at, :].astype(F32)
            earlier = jnp.where(first_row, last_row[j, 0:1, :], pltpu.roll(cur, 1, 0))
            last_row[j] = jnp.broadcast_to(cur[width - 1 :, :], (8, heads * HEAD))
            return cur + (earlier - cur) * mix[j : j + 1, :]

        recept, key, value = shifted(0), shifted(1), shifted(2)
        level = dbase + proj_ref[3, at, :].astype(F32) + drift_ref[b * width]
        logs = -0.6065306597126334 * jax.nn.sigmoid(level)
        rate = jax.nn.sigmoid(rbase + proj_ref[4, at, :].astype(F32))
        total = sum_rows(logs, ones)
        through = jnp.exp(total)
        until = jnp.exp(total - logs)
        inverse = jnp.exp(-total)
        key_s = key * inverse
        rec_s = recept * through
        final = through[width - 1 :, :]
        rate_inv = rate * inverse
        for h in range(heads):
            ch = slice(h * HEAD, (h + 1) * HEAD)
            key_h = key[:, ch]
            unit = key_h * lax.rsqrt(jnp.sum(key_h * key_h, axis=1, keepdims=True) + 1.0)
            val_h = value[:, ch]
            alpha = -unit * until[:, ch]
            beta = unit * rate_inv[:, ch]
            key_sh = key_s[:, ch]
            rec_h = rec_s[:, ch]
            fin = final[:, ch]
            cross = mm(
                jnp.concatenate([alpha, rec_h], axis=0), jnp.concatenate([beta, key_sh], axis=0), NT
            )
            low_ab = jnp.where(strict, cross[:width, :width], 0.0)
            low_ak = jnp.where(strict, cross[:width, width:], 0.0)
            up_b = jnp.where(incl, cross[width:, :width], 0.0)
            up_k = jnp.where(incl, cross[width:, width:], 0.0)
            both = mm(jnp.concatenate([low_ak, up_k], axis=0), val_h)
            inv = eye + jnp.where(levels[0], low_ab, 0.0)
            for mask in levels[1:]:
                inv = inv + mm(inv, mm(jnp.where(mask, low_ab, 0.0), inv))
            solved = mm(inv, jnp.concatenate([alpha, both[:width]], axis=1))
            reads[b, h] = jnp.concatenate([rec_h, both[width:]], axis=1) + mm(up_b, solved)
            ends = jnp.concatenate([beta * fin, key_sh * fin], axis=0)
            piece = mm(
                ends, jnp.concatenate([solved, jnp.concatenate([zeros, val_h], axis=1)], axis=0), TN
            )
            trans = piece[:, :HEAD] + eye * fin
            before = running[h]
            prefix[b, h] = before
            running[h] = mm(trans, before) + jnp.concatenate([zeros, piece[:, HEAD:]], axis=1)

    count = m - 1
    for d in steps:
        count = count + (s + d < n).astype(jnp.int32) + (s - d >= 0).astype(jnp.int32)
    pl.semaphore_wait(barrier, count)

    def joined(later, earlier):
        return mm(later[:, :HEAD], earlier) + jnp.concatenate([zeros, later[:, HEAD:]], axis=1)

    at_start = s == 0
    for h in range(heads):
        own = running[h]
        start = jnp.concatenate([zeros, init_ref[h].T], axis=1)
        window[h] = jnp.where(at_start, start, jnp.concatenate([eye, zeros], axis=1))
        g_buf[0, h] = jnp.where(at_start, joined(own, start), own)

    def hop(k):
        return pltpu.make_async_remote_copy(
            src_ref=g_buf.at[k],
            dst_ref=r_buf.at[k],
            send_sem=g_send.at[k],
            recv_sem=g_recv.at[k],
            device_id={"sp": s + steps[k], "tp": t},
            device_id_type=pl.DeviceIdType.MESH,
        )

    for k, d in enumerate(steps):

        @pl.when(s + d < n)
        def _():
            hop(k).start()

        @pl.when(s - d >= 0)
        def _():
            hop(k).wait_recv()
            for h in range(heads):
                window[h] = joined(window[h], r_buf[k, h])

        if k + 1 < len(steps):
            for h in range(heads):
                g_buf[k + 1, h] = jnp.where(at_start, g_buf[k, h], joined(running[h], window[h]))

    @pl.loop(0, blocks)
    def _(b):
        at = pl.ds(pl.multiple_of(b * width, width), width)
        gate = jax.nn.sigmoid(proj_ref[5, at, :].astype(F32))
        pieces = []
        for h in range(heads):
            ch = slice(h * HEAD, (h + 1) * HEAD)
            now = prefix[b, h]
            state = mm(now[:, :HEAD], window[h][:, HEAD:]) + now[:, HEAD:]
            read = reads[b, h]
            mixed = mm(read[:, :HEAD], state) + read[:, HEAD:]
            center = mixed - jnp.mean(mixed, axis=1, keepdims=True)
            spread = jnp.mean(center * center, axis=1, keepdims=True)
            pieces.append(center * lax.rsqrt(spread + group_floor))
        gated[at, :] = (jnp.concatenate(pieces, axis=1) * gain * gate).astype(BF16)

    share = act.shape[1]

    def part(q):
        dest = lax.rem(t + q, m)
        return pltpu.make_async_remote_copy(
            src_ref=gated.at[pl.ds(pl.multiple_of(dest * share, share), share), :],
            dst_ref=act.at[t],
            send_sem=a_send.at[q],
            recv_sem=a_recv.at[q],
            device_id={"sp": s, "tp": dest},
            device_id_type=pl.DeviceIdType.MESH,
        )

    for q in range(1, m):
        part(q).start()
    act[t] = gated[pl.ds(pl.multiple_of(t * share, share), share), :]
    load.wait()
    for q in range(1, m):
        part(q).wait_recv()
    rows = jnp.concatenate([act[q] for q in range(m)], axis=1)
    columns = out_ref.shape[1]
    tile = min(512, columns)
    for c in range(0, columns, tile):
        out_ref[:, c : c + tile] = dot1(rows, wout[:, c : c + tile], NN).astype(BF16)
    for q in range(1, m):
        part(q).wait_send()
    for k, d in enumerate(steps):

        @pl.when(s + d < n)
        def _():
            hop(k).wait_send()


def scan_call(n, m, drift, proj, edge, mix, dbase, rbase, gain, init, w_out):
    seq, width = proj.shape[1:]
    heads, blocks = width // HEAD, seq // BLOCK
    hops = max(1, (n - 1).bit_length())
    vmem = pl.BlockSpec(memory_space=pltpu.VMEM)
    return pl.pallas_call(
        functools.partial(scan_kernel, n, m, heads, blocks),
        out_shape=jax.ShapeDtypeStruct((seq // m, w_out.shape[1]), BF16),
        in_specs=[pl.BlockSpec(memory_space=pltpu.SMEM)]
        + [vmem] * 7
        + [pl.BlockSpec(memory_space=pl.ANY)],
        out_specs=vmem,
        scratch_shapes=[
            pltpu.VMEM((3, 8, width), F32),
            pltpu.VMEM((blocks, heads, BLOCK, 2 * HEAD), F32),
            pltpu.VMEM((blocks, heads, HEAD, 2 * HEAD), F32),
            pltpu.VMEM((heads, HEAD, 2 * HEAD), F32),
            pltpu.VMEM((heads, HEAD, 2 * HEAD), F32),
            pltpu.VMEM((hops, heads, HEAD, 2 * HEAD), F32),
            pltpu.VMEM((hops, heads, HEAD, 2 * HEAD), F32),
            pltpu.VMEM((8, 128), F32),
            pltpu.VMEM((seq, width), BF16),
            pltpu.VMEM((m, seq // m, width), BF16),
            pltpu.VMEM(w_out.shape, BF16),
            pltpu.SemaphoreType.DMA,
            pltpu.SemaphoreType.DMA((hops,)),
            pltpu.SemaphoreType.DMA((hops,)),
            pltpu.SemaphoreType.DMA((m,)),
            pltpu.SemaphoreType.DMA((m,)),
        ],
        compiler_params=pltpu.CompilerParams(
            collective_id=1, has_side_effects=True, vmem_limit_bytes=48 * 1024 * 1024
        ),
        name="scan_kernel",
    )(drift, proj, edge, mix, dbase, rbase, gain, init, w_out)


def shifted_2(block, axis, distance):
    devices = range(lax.axis_size(axis))
    route = [(i - distance, i) for i in devices if i - distance in devices]
    return lax.ppermute(block, axis, route)


def per_device(
    n,
    m,
    tokens,
    norm_gain,
    w_recept,
    w_key,
    w_value,
    w_decay,
    w_rate,
    w_gate,
    shift_mix,
    decay_base,
    rate_base,
    decay_drift,
    group_gain,
    initial_state,
    w_out,
):
    tok_float = tokens.astype(F32)
    normed = (
        tok_float
        * lax.rsqrt(jnp.mean(tok_float * tok_float, axis=-1, keepdims=True) + norm_floor)
        * norm_gain
    ).astype(BF16)
    weights = (w_recept, w_key, w_value, w_decay, w_rate, w_gate)
    piece = lax.all_gather(normed, "tp", axis=0, tiled=True)
    projected = jnp.stack(
        [jnp.dot(piece, weight, preferred_element_type=F32).astype(BF16) for weight in weights], axis=0
    )
    edge = shifted_2(projected[0:3, -1:, :], "sp", 1)
    return scan_call(
        n, m, decay_drift, projected, edge, shift_mix, decay_base, rate_base, group_gain, initial_state, w_out
    )


def solution(mesh):
    return jax.shard_map(
        functools.partial(per_device, mesh.shape["sp"], mesh.shape["tp"]),
        mesh=mesh,
        in_specs=(
            P(("sp", "tp"), None),
            P(),
            P(None, "tp"),
            P(None, "tp"),
            P(None, "tp"),
            P(None, "tp"),
            P(None, "tp"),
            P(None, "tp"),
            P(None, "tp"),
            P("tp"),
            P("tp"),
            P("sp"),
            P("tp"),
            P("tp", None, None),
            P(),
        ),
        out_specs=P(("sp", "tp"), None),
        check_vma=False,
    )
```

time: 327 us -> 126 us (0.39); the launches traced: 323 us -> 125 us
  other arithmetic: 130 us -> 3.18 us
  Pallas kernels: 0 us -> 78.1 us
  blocking collectives: 75.5 us -> 0 us
  matrix products: 59.8 us -> 4.97 us
  local copies, waits for them, and re-layouts: 23.2 us -> 2.54 us
  waiting for transfers between devices: 17.7 us -> 21.7 us
    another operation x4 -> x1, other arithmetic: 121 us -> 0.01 us  [per_device(): jnp.stack([jnp.dot(piece, weight, preferred_element_type=F32).astype(BF16...]
    pallas_call x0 -> x1, Pallas kernels: none -> 78.1 us  [scan_call(): pl.pallas_call(functools.partial(scan_kernel, n, m, heads, blocks), out_s...]
    all_gather x2 -> x0, blocking collectives: 57.1 us -> none  [carried_in(): pieces = jax.tree.map(lambda part: lax.all_gather(part, axis), value)]
    dot_general x46 -> x6, matrix products: 58.2 us -> 4.97 us  [per_device(): jnp.dot(piece, weight, preferred_element_type=F32).astype(BF16)]
    all_to_all x1 -> x0, blocking collectives: 18.4 us -> none  [per_device(): lax.all_to_all(gated, 'tp', split_axis=0, concat_axis=1, tiled=True)]
    dynamic_slice x14 -> x0, local copies, waits for them, and re-layouts: 7.11 us -> none  [turn(): longer = join(running, jax.tree.map(lambda part: part[position], pieces))]
    another operation x3 -> x0, local copies, waits for them, and re-layouts: 4.86 us -> none  [the longest x2 3.54 us: blocked(): array.reshape(block_count, BLOCK, local_heads, HEAD).transpose(0, 2, 1, 3)]
    all_gather x1, waiting for transfers between devices: 17.7 us -> 21.1 us  [per_device(): piece = lax.all_gather(normed, 'tp', axis=0, tiled=True)]
  transfers between devices with their start and end apart: 2 -> 2, of which waited for: 1 -> 2; matrix products, arithmetic and copies ran while one was open for 3% -> 1% of each run, Pallas kernels for 0% -> 0%
where the time goes in v1:
time: 126 us; the launch traced here: 125 us
  Pallas kernels  78.1 us (62%)
  waiting for transfers between devices  21.7 us (17%)
  between operations  13.6 us (11%)
  matrix products  4.97 us (4%)
  other arithmetic  3.18 us (3%)
  local copies, waits for them, and re-layouts  2.54 us (2%)
  starting transfers between devices  1.29 us (1%)
    pallas_call x1, Pallas kernels, scan_call(): pl.pallas_call(functools.partial(scan_kernel, n, m, heads, blocks), out_s...  78.1 us
    all_gather x1, waiting for transfers between devices, per_device(): piece = lax.all_gather(normed, 'tp', axis=0, tiled=True)  21.1 us
    dot_general x6, matrix products, per_device(): jnp.dot(piece, weight, preferred_element_type=F32).astype(BF16)  4.97 us
    unnamed x29, local copies, waits for them, and re-layouts  2.54 us
  transfers between devices with their start and end apart: 2, of which 2 were waited for; matrix products, arithmetic and copies ran while one was open for 1% of the time, Pallas kernels for 0%

profile of v1, /device:TPU:27, one launch (start us, length us, event | category | flops | bytes accessed | tf_op | source)
XLA Modules:
  0.0 125.4 jit_solution(4568860602329003532)
XLA Ops:
  6.5 0.0 copy-start
  6.5 0.0 all-gather.2.cloned.1.call-start
  6.5 1.3 %fusion.9 = f32[96]{0:T(128)S(1)} fusion(bf16[96,2048]{1,0:T(8,128)(2,1)} %param.15), kind=kLoop, calls=%fused_computation.17 | loop fusion | flops 589728 | bytes 393600 | tf_op jit(solution)/shard_map/reduce_sum | solution.py:334
  7.8 1.9 %fusion.11 = bf16[96,2048]{1,0:T(8,128)(2,1)} fusion(bf16[96,2048]{1,0:T(8,128)(2,1)} %param.15, f32[2048]{0:T(1024)} %param.16, f32[96]{0:T(128)S(1)} %add_rsqrt_fusion), kind=kLoop, calls=%fused_computation.19 | loop fusion | flops 786432 | bytes 795008 | tf_op jit(solution)/shard_map/convert_element_type | solution.py:336
  9.7 0.0 all-gather.2.cloned.1.call-update
  9.8 0.0 copy-start.9
  9.8 21.1 %all-gather.2.cloned.1.call-done = bf16[384,2048]{1,0:T(8,128)(2,1)} async-done(((bf16[96,2048]{1,0:T(8,128)(2,1)}), bf16[384,2048]{1,0:T(8,128)(2,1)}) %all-gather.2.cloned.1.call-update) | async-done | bytes 1572880 | tf_op jit(solution)/shard_map/all_gather | solution.py:338
  30.9 0.0 copy-done
  30.9 0.0 copy-start.8
  30.9 2.1 %constant_dynamic-update-slice_fusion.2 = (bf16[6,384,256]{2,1,0:T(8,128)(2,1)S(1)}, bf16[1,384,256]{2,1,0:T(8,128)(2,1)S(1)}) fusion(bf16[384,2048]{1,0:T(8,128)(2,1)} %all-gather.2.cloned.1.call-done, bf16[2048,256]{1,0:T(8,128)(2,1)S(1)} %copy-done), kind=kOutput, calls=%fused_computation.22 | convolution fusion | flops 402751488 | bytes 3014656 | tf_op jit(solution)/shard_map/dot_general | solution.py:340
  33.0 0.0 copy-done.9
  33.0 0.0 copy-done.8
  33.0 0.0 copy-start.10
  33.0 0.6 constant_dynamic-update-slice_fusion.1
  33.6 0.6 copy-done.10
  34.2 0.0 copy-start.11
  34.2 0.6 constant_dynamic-update-slice_fusion
  34.8 1.3 %collective-permute-start = (bf16[3,1,256]{2,1,0:T(2,128)(2,1)S(1)}, bf16[3,1,256]{2,1,0:T(2,128)(2,1)S(1)}, u32[]{:S(2)}, u32[]{:S(2)}) collective-permute-start(bf16[3,1,256]{2,1,0:T(2,128)(2,1)S(1)} %pad_maximum_fusion), channel_id=1, source_target_pairs={{0,4},{4,8},{8,12},{12,16},{16,20},{20,24},{24,28},{1,5},{5,9},{9,... | collective-permute-start | bytes 4616 | tf_op jit(solution)/shard_map/ppermute | solution.py:309
  36.1 0.0 copy-done.11
  36.2 0.0 copy-start.12
  36.2 0.0 copy-start.13
  36.2 0.6 fusion.4
  36.8 0.6 copy-done.12
  37.4 0.0 copy-start.1
  37.4 0.6 fusion.6
  38.0 0.0 copy-done.13
  38.0 0.0 copy-start.2
  38.0 0.0 copy-start.3
  38.0 0.0 copy-start.4
  38.0 0.0 copy-start.5
  38.0 0.0 copy-start.6
  38.0 0.0 copy-start.7
  38.0 0.6 fusion.8.proj_ref
  38.6 0.6 collective-permute-done.edge_ref
  39.2 0.5 copy-done.1
  39.7 0.0 copy-done.2
  39.7 0.0 copy-done.3
  39.7 0.0 copy-done.4
  39.7 0.0 copy-done.5
  39.7 0.0 copy-done.6
  39.7 0.0 copy-done.7
  39.7 78.1 %scan_kernel.1 = bf16[96,2048]{1,0:T(8,128)(2,1)S(1)} custom-call(f32[384]{0:T(512)S(1)} %copy-done.4, bf16[6,384,256]{2,1,0:T(8,128)(2,1)S(1)} %fusion.8.proj_ref, bf16[3,1,256]{2,1,0:T(2,128)(2,1)S(1)} %collective-permute-done.edge_ref, f32[3,256]{1,0:T(4,128)S(1)} %copy-done.3, f32[256]{0:T(256)S(1)} %copy-done.5, f32[256]{0:T(256)S(1)} %copy-done.6, ...), custom_call_target="tpu_custom_call" | custom-call | tf_op jit(solution)/shard_map/scan_kernel/pallas_call | solution.py:274
  117.8 0.7 copy.22
  (2 shorter events, 0.0 us)
Async XLA Ops:
  6.5 24.4 %copy-start = (bf16[2048,256]{1,0:T(8,128)(2,1)S(1)}, bf16[2048,256]{1,0:T(8,128)(2,1)}, u32[]{:S(2)}) copy-start(bf16[2048,256]{1,0:T(8,128)(2,1)} %param.17) | copy-start | bytes 3145732
  6.5 24.4 %all-gather.2.cloned.1.call-start = ((), (), s32[]{:S(2)}) async-start(), calls=%async_computation | async-start | bytes 1966080 | tf_op jit(solution)/shard_map/all_gather | solution.py:338
  9.8 23.2 %copy-start.9 = (bf16[2048,256]{1,0:T(8,128)(2,1)S(1)}, bf16[2048,256]{1,0:T(8,128)(2,1)}, u32[]{:S(2)}) copy-start(bf16[2048,256]{1,0:T(8,128)(2,1)} %param.18) | copy-start | bytes 3145732
  30.9 2.1 %copy-start.8 = (bf16[384,2048]{1,0:T(8,128)(2,1)S(1)}, bf16[384,2048]{1,0:T(8,128)(2,1)}, u32[]{:S(2)}) copy-start(bf16[384,2048]{1,0:T(8,128)(2,1)} %all-gather.2.cloned.1.call-done) | copy-start | bytes 4718596
  33.0 1.2 copy-start.10
  34.2 1.9 %copy-start.11 = (bf16[2048,256]{1,0:T(8,128)(2,1)S(1)}, bf16[2048,256]{1,0:T(8,128)(2,1)}, u32[]{:S(2)}) copy-start(bf16[2048,256]{1,0:T(8,128)(2,1)} %param.20) | copy-start | bytes 3145732
  34.8 4.3 %collective-permute-start = (bf16[3,1,256]{2,1,0:T(2,128)(2,1)S(1)}, bf16[3,1,256]{2,1,0:T(2,128)(2,1)S(1)}, u32[]{:S(2)}, u32[]{:S(2)}) collective-permute-start(bf16[3,1,256]{2,1,0:T(2,128)(2,1)S(1)} %pad_maximum_fusion), channel_id=1, source_target_pairs={{0,4},{4,8},{8,12},{12,16},{16,20},{20,24},{24,28},{1,5},{5,9},{9,... | collective-permute-start | bytes 4616 | tf_op jit(solution)/shard_map/ppermute | solution.py:309
  36.2 1.2 copy-start.12
  36.2 1.8 %copy-start.13 = (bf16[2048,256]{1,0:T(8,128)(2,1)S(1)}, bf16[2048,256]{1,0:T(8,128)(2,1)}, u32[]{:S(2)}) copy-start(bf16[2048,256]{1,0:T(8,128)(2,1)} %param.22) | copy-start | bytes 3145732
  37.4 2.3 %copy-start.1 = (bf16[1024,2048]{1,0:T(8,128)(2,1)S(1)}, bf16[1024,2048]{1,0:T(8,128)(2,1)}, u32[]{:S(2)}) copy-start(bf16[1024,2048]{1,0:T(8,128)(2,1)} %wout_ref.1) | copy-start | bytes 12582916
  38.0 1.7 %copy-start.2 = (f32[4,64,64]{2,1,0:T(8,128)S(1)}, f32[4,64,64]{2,1,0:T(8,128)}, u32[]{:S(2)}) copy-start(f32[4,64,64]{2,1,0:T(8,128)} %init_ref.1) | copy-start | bytes 196612
  38.0 1.7 %copy-start.3 = (f32[3,256]{1,0:T(4,128)S(1)}, f32[3,256]{1,0:T(4,128)}, u32[]{:S(2)}) copy-start(f32[3,256]{1,0:T(4,128)} %mix_ref.1) | copy-start | bytes 9220
  38.0 1.7 %copy-start.4 = (f32[384]{0:T(512)S(1)}, f32[384]{0:T(512)}, u32[]{:S(2)}) copy-start(f32[384]{0:T(512)} %drift_ref.1) | copy-start | bytes 4612
  38.0 1.7 %copy-start.5 = (f32[256]{0:T(256)S(1)}, f32[256]{0:T(256)}, u32[]{:S(2)}) copy-start(f32[256]{0:T(256)} %dbase_ref.1) | copy-start | bytes 3076
  38.0 1.6 %copy-start.6 = (f32[256]{0:T(256)S(1)}, f32[256]{0:T(256)}, u32[]{:S(2)}) copy-start(f32[256]{0:T(256)} %rbase_ref.1) | copy-start | bytes 3076
  38.0 1.6 %copy-start.7 = (f32[256]{0:T(256)S(1)}, f32[256]{0:T(256)}, u32[]{:S(2)}) copy-start(f32[256]{0:T(256)} %gain_ref.1) | copy-start | bytes 3076
Sparse Core Ops, SparseCore 0:
  9.9 20.9 all-gather.1

commit v2 on v1

v2 whole, which is shorter than its diff:
```python
import functools

import jax
import jax.numpy as jnp
from jax import lax
from jax.experimental import pallas as pl
from jax.experimental.pallas import tpu as pltpu
from jax.sharding import PartitionSpec as P

HEAD = 64
BLOCK = 64
F32 = jnp.float32
BF16 = jnp.bfloat16

norm_floor = 0.5
group_floor = 1.0

NN = (((1,), (0,)), ((), ()))
NT = (((1,), (1,)), ((), ()))
TN = (((0,), (0,)), ((), ()))


def dot1(a, b, dims):
    return lax.dot_general(a, b, dims, preferred_element_type=F32)


def split(a):
    high = a.astype(BF16)
    return high, (a - high.astype(F32)).astype(BF16)


def mm(a, b, dims=NN):
    ah, al = split(a)
    bh, bl = split(b)
    return dot1(ah, bh, dims) + (dot1(ah, bl, dims) + dot1(al, bh, dims))


def sum_rows(a, ones):
    high, rest = split(a)
    mid, low = split(a - high.astype(F32))
    return dot1(ones, high, NN) + (dot1(ones, mid, NN) + dot1(ones, low, NN))


def layer_kernel(
    n,
    m,
    heads,
    blocks,
    drift_ref,
    tok_ref,
    ngain_ref,
    wr_ref,
    wk_ref,
    wv_ref,
    wd_ref,
    wa_ref,
    wg_ref,
    mix_ref,
    dbase_ref,
    rbase_ref,
    gain_ref,
    init_ref,
    wout_ref,
    out_ref,
    tok,
    edge_out,
    edge_in,
    normed,
    weights,
    proj,
    edges,
    last_row,
    reads,
    pieces,
    prefix,
    running,
    window,
    g_buf,
    r_buf,
    gated,
    act,
    wout,
    own_sem,
    w_sem,
    t_send,
    t_recv,
    f_send,
    f_recv,
    e_send,
    e_recv,
    g_send,
    g_recv,
    a_send,
    a_recv,
):
    s = lax.axis_index("sp")
    t = lax.axis_index("tp")
    half = m // 2
    upper = t // half
    base = upper * half
    across = lax.rem(t + half, m)
    share, depth = tok_ref.shape
    lanes = edge_out.shape[1]
    width = BLOCK
    channels = heads * HEAD
    steps = []
    while (1 << len(steps)) < n:
        steps.append(1 << len(steps))

    def near(q):
        return base + lax.rem(t - base + q, half)

    own_load = pltpu.make_async_copy(tok_ref, tok.at[t], own_sem)
    own_load.start()
    sources = (wr_ref, wk_ref, wv_ref, wd_ref, wa_ref, wg_ref)
    loads = [
        pltpu.make_async_copy(ref, weights.at[j], w_sem.at[j]) for j, ref in enumerate(sources)
    ]
    for load in loads:
        load.start()
    out_load = pltpu.make_async_copy(wout_ref, wout, w_sem.at[len(sources)])
    out_load.start()

    barrier = pltpu.get_barrier_semaphore()
    count = m - 1

    def greet(sp, tp):
        pl.semaphore_signal(
            barrier, inc=1, device_id={"sp": sp, "tp": tp}, device_id_type=pl.DeviceIdType.MESH
        )

    for q in range(1, m):
        greet(s, lax.rem(t + q, m))
    for d in steps:
        for other, ok in ((s + d, s + d < n), (s - d, s - d >= 0)):
            count = count + ok.astype(jnp.int32)

            @pl.when(ok)
            def _():
                greet(other, t)

    for q in range(m - 1):
        sends = jnp.logical_and(t == m - 1, s + 1 < n)
        takes = jnp.logical_and(t == q, s >= 1)
        count = count + sends.astype(jnp.int32) + takes.astype(jnp.int32)

        @pl.when(sends)
        def _():
            greet(s + 1, q)

        @pl.when(takes)
        def _():
            greet(s - 1, m - 1)

    own_load.wait()
    last = tok[t, share - 16 :, :].astype(F32)[15:16, :]
    for i in range(depth // lanes):
        edge_out[i : i + 1, :] = last[:, i * lanes : (i + 1) * lanes]
    pl.semaphore_wait(barrier, count)

    def remote(src, dst, send, recv, sp, tp):
        return pltpu.make_async_remote_copy(
            src_ref=src,
            dst_ref=dst,
            send_sem=send,
            recv_sem=recv,
            device_id={"sp": sp, "tp": tp},
            device_id_type=pl.DeviceIdType.MESH,
        )

    def token_copy(q):
        other = across if q == 0 else near(q)
        return remote(tok.at[t], tok.at[t], t_send.at[q], t_recv.at[q], s, other)

    def forward_copy(q):
        return remote(tok.at[across], tok.at[across], f_send.at[q], f_recv.at[q], s, near(q))

    def edge_copy(q):
        return remote(edge_out, edge_in.at[0], e_send.at[q], e_recv.at[0], s + 1, q)

    def middle_copy(q):
        return remote(edge_out, edge_in.at[1], e_send.at[q], e_recv.at[1], s, half + q)

    has_next = jnp.logical_and(t == m - 1, s + 1 < n)
    has_middle = t == half - 1

    @pl.when(has_next)
    def _():
        for q in range(m):
            edge_copy(q).start()

    @pl.when(has_middle)
    def _():
        for q in range(half):
            middle_copy(q).start()

    for q in range(half):
        token_copy(q).start()

    rows_i = lax.broadcasted_iota(jnp.int32, (width, width), 0)
    cols_i = lax.broadcasted_iota(jnp.int32, (width, width), 1)
    strict = cols_i < rows_i
    incl = cols_i <= rows_i
    eye = jnp.where(cols_i == rows_i, 1.0, 0.0).astype(F32)
    ones = jnp.where(incl, 1.0, 0.0).astype(BF16)
    zeros = jnp.zeros((width, HEAD), F32)
    levels = []
    size = 1
    while size < width:
        same = (rows_i // (2 * size)) == (cols_i // (2 * size))
        levels.append(same & ((rows_i // size) % 2 == 1) & ((cols_i // size) % 2 == 0))
        size *= 2
    first_row = lax.broadcasted_iota(jnp.int32, (width, channels), 0) == 0
    mix = mix_ref[...]
    dbase = dbase_ref[...].reshape(1, channels)
    rbase = rbase_ref[...].reshape(1, channels)
    gain = gain_ref[...].reshape(1, channels)
    ngain = ngain_ref[...].reshape(1, depth)

    def norm(x):
        scale = lax.rsqrt(jnp.mean(x * x, axis=1, keepdims=True) + norm_floor)
        return (x * scale * ngain).astype(BF16)

    tile = 32
    span = half * share

    def norm_block(owner, place):
        @pl.loop(0, share // tile)
        def _(i):
            rows = pl.ds(pl.multiple_of(i * tile, tile), tile)
            to = pl.ds(pl.multiple_of(place * share + i * tile, tile), tile)
            normed[to, :] = norm(tok[owner, rows, :].astype(F32))

    def project(first, extra):
        to = pl.ds(pl.multiple_of(first * share, share), span)
        for j in range(len(sources)):
            if extra:
                loads[j].wait()
            if extra and j < 3:
                made = dot1(normed[...], weights[j], NN).astype(BF16)
                edges[j] = made[span:, :].astype(F32)
                proj[j, to, :] = made[:span, :]
            else:
                proj[j, to, :] = dot1(normed[:span, :], weights[j], NN).astype(BF16)

    def prepare(b):
        at = pl.ds(pl.multiple_of(b * width, width), width)

        def shifted(j):
            cur = proj[j, at, :].astype(F32)
            earlier = jnp.where(first_row, last_row[j, 0:1, :], pltpu.roll(cur, 1, 0))
            last_row[j] = jnp.broadcast_to(cur[width - 1 :, :], (8, channels))
            return cur + (earlier - cur) * mix[j : j + 1, :]

        recept, key, value = shifted(0), shifted(1), shifted(2)
        level = dbase + proj[3, at, :].astype(F32) + drift_ref[b * width]
        logs = -0.6065306597126334 * jax.nn.sigmoid(level)
        rate = jax.nn.sigmoid(rbase + proj[4, at, :].astype(F32))
        total = sum_rows(logs, ones)
        through = jnp.exp(total)
        until = jnp.exp(total - logs)
        inverse = jnp.exp(-total)
        key_s = key * inverse
        rec_s = recept * through
        final = through[width - 1 :, :]
        rate_inv = rate * inverse
        every = range(heads)
        chans = [slice(h * HEAD, (h + 1) * HEAD) for h in every]
        units = []
        for ch in chans:
            key_h = key[:, ch]
            units.append(key_h * lax.rsqrt(jnp.sum(key_h * key_h, axis=1, keepdims=True) + 1.0))
        alphas = [-units[h] * until[:, chans[h]] for h in every]
        betas = [units[h] * rate_inv[:, chans[h]] for h in every]
        keys = [key_s[:, ch] for ch in chans]
        recs = [rec_s[:, ch] for ch in chans]
        vals = [value[:, ch] for ch in chans]
        fins = [final[:, ch] for ch in chans]
        cross = [
            mm(
                jnp.concatenate([alphas[h], recs[h]], axis=0),
                jnp.concatenate([betas[h], keys[h]], axis=0),
                NT,
            )
            for h in every
        ]
        low_ab = [jnp.where(strict, c[:width, :width], 0.0) for c in cross]
        low_ak = [jnp.where(strict, c[:width, width:], 0.0) for c in cross]
        up_b = [jnp.where(incl, c[width:, :width], 0.0) for c in cross]
        up_k = [jnp.where(incl, c[width:, width:], 0.0) for c in cross]
        both = [mm(jnp.concatenate([low_ak[h], up_k[h]], axis=0), vals[h]) for h in every]
        inv = [eye + jnp.where(levels[0], low, 0.0) for low in low_ab]
        for mask in levels[1:]:
            right = [mm(jnp.where(mask, low_ab[h], 0.0), inv[h]) for h in every]
            inv = [inv[h] + mm(inv[h], right[h]) for h in every]
        solved = [
            mm(inv[h], jnp.concatenate([alphas[h], both[h][:width]], axis=1)) for h in every
        ]
        for h in every:
            reads[b, h] = jnp.concatenate([recs[h], both[h][width:]], axis=1) + mm(
                up_b[h], solved[h]
            )
        for h in every:
            ends = jnp.concatenate([betas[h] * fins[h], keys[h] * fins[h]], axis=0)
            piece = mm(
                ends,
                jnp.concatenate(
                    [solved[h], jnp.concatenate([zeros, vals[h]], axis=1)], axis=0
                ),
                TN,
            )
            pieces[b, h] = piece + jnp.concatenate([eye * fins[h], zeros], axis=1)

    def open_half(which):
        for j in range(3):
            row = jnp.where(which == 0, edges[j, 0:1, :], edges[j, 1:2, :])
            last_row[j] = jnp.broadcast_to(row, (8, channels))

    norm_block(t, t - base)
    for q in range(1, half):
        token_copy(q).wait_recv()
        norm_block(near(half - q), near(half - q) - base)

    @pl.when(s >= 1)
    def _():
        remote(edge_out, edge_in.at[0], e_send.at[0], e_recv.at[0], s, t).wait_recv()

    @pl.when(s == 0)
    def _():
        edge_in[0] = jnp.zeros(edge_in.shape[1:], F32)

    @pl.when(upper == 1)
    def _():
        remote(edge_out, edge_in.at[1], e_send.at[0], e_recv.at[1], s, t).wait_recv()

    @pl.when(upper == 0)
    def _():
        row = tok[half - 1, share - 16 :, :].astype(F32)[15:16, :]
        for i in range(depth // lanes):
            edge_in[1, i : i + 1, :] = row[:, i * lanes : (i + 1) * lanes]

    joined_rows = [
        jnp.concatenate([edge_in[k, i : i + 1, :] for i in range(depth // lanes)], axis=1)
        for k in range(2)
    ]
    normed[span:, :] = norm(
        jnp.concatenate(joined_rows + [jnp.zeros((14, depth), F32)], axis=0)
    )
    project(base, True)
    open_half(upper)

    @pl.loop(0, blocks // 2)
    def _(i):
        prepare(upper * (blocks // 2) + i)

        @pl.when(i == 0)
        def _():
            token_copy(0).wait_recv()
            for q in range(1, half):
                forward_copy(q).start()

    lower = 1 - upper
    norm_block(across, across - lower * half)
    for q in range(1, half):
        forward_copy(q).wait_recv()
        far = lower * half + near(half - q) - base
        norm_block(far, far - lower * half)
    project(lower * half, False)
    open_half(lower)

    @pl.loop(0, blocks // 2)
    def _(i):
        prepare(lower * (blocks // 2) + i)

    def joined(later, earlier):
        return mm(later[:, :HEAD], earlier) + jnp.concatenate([zeros, later[:, HEAD:]], axis=1)

    for h in range(heads):
        running[h] = jnp.concatenate([eye, zeros], axis=1)

    @pl.loop(0, blocks)
    def _(b):
        for h in range(heads):
            prefix[b, h] = running[h]
            running[h] = joined(pieces[b, h], running[h])

    at_start = s == 0
    for h in range(heads):
        own = running[h]
        start = jnp.concatenate([zeros, init_ref[h].T], axis=1)
        window[h] = jnp.where(at_start, start, jnp.concatenate([eye, zeros], axis=1))
        g_buf[0, h] = jnp.where(at_start, joined(own, start), own)

    def hop(k):
        return remote(g_buf.at[k], r_buf.at[k], g_send.at[k], g_recv.at[k], s + steps[k], t)

    for k, d in enumerate(steps):

        @pl.when(s + d < n)
        def _():
            hop(k).start()

        @pl.when(s - d >= 0)
        def _():
            hop(k).wait_recv()
            for h in range(heads):
                window[h] = joined(window[h], r_buf[k, h])

        if k + 1 < len(steps):
            for h in range(heads):
                g_buf[k + 1, h] = jnp.where(at_start, g_buf[k, h], joined(running[h], window[h]))

    @pl.loop(0, blocks)
    def _(b):
        at = pl.ds(pl.multiple_of(b * width, width), width)
        gate = jax.nn.sigmoid(proj[5, at, :].astype(F32))
        parts = []
        for h in range(heads):
            now = prefix[b, h]
            state = mm(now[:, :HEAD], window[h][:, HEAD:]) + now[:, HEAD:]
            read = reads[b, h]
            mixed = mm(read[:, :HEAD], state) + read[:, HEAD:]
            center = mixed - jnp.mean(mixed, axis=1, keepdims=True)
            spread = jnp.mean(center * center, axis=1, keepdims=True)
            parts.append(center * lax.rsqrt(spread + group_floor))
        gated[at, :] = (jnp.concatenate(parts, axis=1) * gain * gate).astype(BF16)

    def part(q):
        dest = lax.rem(t + q, m)
        rows = pl.ds(pl.multiple_of(dest * share, share), share)
        return remote(gated.at[rows, :], act.at[t], a_send.at[q], a_recv.at[q], s, dest)

    for q in range(1, m):
        part(q).start()
    act[t] = gated[pl.ds(pl.multiple_of(t * share, share), share), :]
    out_load.wait()
    for q in range(1, m):
        part(q).wait_recv()
    rows = jnp.concatenate([act[q] for q in range(m)], axis=1)
    columns = out_ref.shape[1]
    out_tile = min(512, columns)
    for c in range(0, columns, out_tile):
        out_ref[:, c : c + out_tile] = dot1(rows, wout[:, c : c + out_tile], NN).astype(BF16)
    for q in range(1, m):
        part(q).wait_send()
    for q in range(half):
        token_copy(q).wait_send()
    for q in range(1, half):
        forward_copy(q).wait_send()

    @pl.when(has_next)
    def _():
        for q in range(m):
            edge_copy(q).wait_send()

    @pl.when(has_middle)
    def _():
        for q in range(half):
            middle_copy(q).wait_send()

    for k, d in enumerate(steps):

        @pl.when(s + d < n)
        def _():
            hop(k).wait_send()


def per_device(
    n,
    m,
    tokens,
    norm_gain,
    w_recept,
    w_key,
    w_value,
    w_decay,
    w_rate,
    w_gate,
    shift_mix,
    decay_base,
    rate_base,
    decay_drift,
    group_gain,
    initial_state,
    w_out,
):
    share, depth = tokens.shape
    width = w_recept.shape[1]
    seq = share * m
    span = share * m // 2
    heads, blocks = width // HEAD, seq // BLOCK
    hops = max(1, (n - 1).bit_length())
    lanes = 128
    vmem = pl.BlockSpec(memory_space=pltpu.VMEM)
    anywhere = pl.BlockSpec(memory_space=pl.ANY)
    dma = pltpu.SemaphoreType.DMA
    return pl.pallas_call(
        functools.partial(layer_kernel, n, m, heads, blocks),
        out_shape=jax.ShapeDtypeStruct((share, w_out.shape[1]), BF16),
        in_specs=[pl.BlockSpec(memory_space=pltpu.SMEM), anywhere, vmem]
        + [anywhere] * 6
        + [vmem] * 5
        + [anywhere],
        out_specs=vmem,
        scratch_shapes=[
            pltpu.VMEM((m, share, depth), BF16),
            pltpu.VMEM((depth // lanes, lanes), F32),
            pltpu.VMEM((2, depth // lanes, lanes), F32),
            pltpu.VMEM((span + 16, depth), BF16),
            pltpu.VMEM((6, depth, width), BF16),
            pltpu.VMEM((6, seq, width), BF16),
            pltpu.VMEM((3, 16, width), F32),
            pltpu.VMEM((3, 8, width), F32),
            pltpu.VMEM((blocks, heads, BLOCK, 2 * HEAD), F32),
            pltpu.VMEM((blocks, heads, HEAD, 2 * HEAD), F32),
            pltpu.VMEM((blocks, heads, HEAD, 2 * HEAD), F32),
            pltpu.VMEM((heads, HEAD, 2 * HEAD), F32),
            pltpu.VMEM((heads, HEAD, 2 * HEAD), F32),
            pltpu.VMEM((hops, heads, HEAD, 2 * HEAD), F32),
            pltpu.VMEM((hops, heads, HEAD, 2 * HEAD), F32),
            pltpu.VMEM((seq, width), BF16),
            pltpu.VMEM((m, share, width), BF16),
            pltpu.VMEM(w_out.shape, BF16),
            dma,
            dma((7,)),
            dma((m,)),
            dma((m,)),
            dma((m,)),
            dma((m,)),
            dma((m,)),
            dma((2,)),
            dma((hops,)),
            dma((hops,)),
            dma((m,)),
            dma((m,)),
        ],
        compiler_params=pltpu.CompilerParams(
            collective_id=1, has_side_effects=True, vmem_limit_bytes=60 * 1024 * 1024
        ),
        name="layer_kernel",
    )(
        decay_drift,
        tokens,
        norm_gain,
        w_recept,
        w_key,
        w_value,
        w_decay,
        w_rate,
        w_gate,
        shift_mix,
        decay_base,
        rate_base,
        group_gain,
        initial_state,
        w_out,
    )


def solution(mesh):
    return jax.shard_map(
        functools.partial(per_device, mesh.shape["sp"], mesh.shape["tp"]),
        mesh=mesh,
        in_specs=(
            P(("sp", "tp"), None),
            P(),
            P(None, "tp"),
            P(None, "tp"),
            P(None, "tp"),
            P(None, "tp"),
            P(None, "tp"),
            P(None, "tp"),
            P(None, "tp"),
            P("tp"),
            P("tp"),
            P("sp"),
            P("tp"),
            P("tp", None, None),
            P(),
        ),
        out_specs=P(("sp", "tp"), None),
        check_vma=False,
    )
```

time: 126 us -> 56.8 us (0.45)
  Pallas kernels: 78.1 us -> 54.9 us
  waiting for transfers between devices: 21.7 us -> 0 us
  between operations: 13.6 us -> 0.01 us
  matrix products: 4.97 us -> 0 us
  other arithmetic: 3.18 us -> 0 us
  starting transfers between devices: 1.29 us -> 0 us
    pallas_call x1, Pallas kernels: 78.1 us -> 54.9 us  [per_device(): pl.pallas_call(functools.partial(layer_kernel, n, m, heads, blocks), out_...]
    all_gather x1 -> x0, waiting for transfers between devices: 21.1 us -> none  [per_device(): piece = lax.all_gather(normed, 'tp', axis=0, tiled=True)]
    dot_general x6 -> x0, matrix products: 4.97 us -> none  [per_device(): jnp.dot(piece, weight, preferred_element_type=F32).astype(BF16)]
    convert_element_type x1 -> x0, other arithmetic: 1.91 us -> none  [per_device(): normed = (tok_float * lax.rsqrt(jnp.mean(tok_float * tok_float, axis=-1,...]
    ppermute x1 -> x0, starting transfers between devices: 1.29 us -> none  [shifted_2(): return lax.ppermute(block, axis, route)]
    unnamed x29 -> x1, local copies, waits for them, and re-layouts: 2.54 us -> 1.77 us
  transfers between devices with their start and end apart: 2 -> 0, of which waited for: 2 -> 0; matrix products, arithmetic and copies ran while one was open for 1% -> 0% of each run, Pallas kernels for 0% -> 0%
where the time goes in v2:
time: 56.8 us; the launch traced here: 56.7 us
  Pallas kernels  54.9 us (97%)
  local copies, waits for them, and re-layouts  1.77 us (3%)
    pallas_call x1, Pallas kernels, per_device(): pl.pallas_call(functools.partial(layer_kernel, n, m, heads, blocks), out_...  54.9 us
    unnamed x1, local copies, waits for them, and re-layouts  1.77 us

profile of v2, /device:TPU:27, one launch (start us, length us, event | category | flops | bytes accessed | tf_op | source)
XLA Modules:
  0.0 56.7 jit_solution(5337476434505868809)
XLA Ops:
  0.0 54.9 %layer_kernel.1 = bf16[96,2048]{1,0:T(8,128)(2,1)} custom-call(f32[384]{0:T(512)} %drift_ref.1, bf16[96,2048]{1,0:T(8,128)(2,1)} %tok_ref.1, f32[2048]{0:T(1024)} %ngain_ref.1, bf16[2048,256]{1,0:T(8,128)(2,1)} %wr_ref.1, bf16[2048,256]{1,0:T(8,128)(2,1)} %wk_ref.1, bf16[2048,256]{1,0:T(8,128)(2,1)} %wv_ref.1, bf16[2048,256]{1,0:T(8,128)(2,1)} %wd_ref.1, ...), custom_call_target="tpu_custom_call" | custom-call | tf_op jit(solution)/shard_map/layer_kernel/pallas_call | solution.py:497
  54.9 1.8 %copy.17 = bf16[96,2048]{1,0:T(8,128)(2,1)} copy(bf16[96,2048]{1,0:T(8,128)(2,1)} %layer_kernel.1) | data formatting | bytes 786432

commit v3 on v2

--- a/solution.py
+++ b/solution.py
@@ -35,10 +35,23 @@
     return dot1(ah, bh, dims) + (dot1(ah, bl, dims) + dot1(al, bh, dims))
 
 
+def mm1(a, b, dims=NN):
+    return dot1(a.astype(BF16), b.astype(BF16), dims)
+
+
+def mm2(a, b, dims=NN):
+    ah, al = split(a)
+    return dot1(ah, b, dims) + dot1(al, b, dims)
+
+
 def sum_rows(a, ones):
     high, rest = split(a)
     mid, low = split(a - high.astype(F32))
     return dot1(ones, high, NN) + (dot1(ones, mid, NN) + dot1(ones, low, NN))
+
+
+def chunks_of(share):
+    return max(c for c in (1, 2, 3, 4) if share % (16 * c) == 0)
 
 
 def layer_kernel(
@@ -71,6 +84,10 @@
     edges,
     last_row,
     reads,
+    ups,
+    stack,
+    final_reads,
+    gates,
     pieces,
     prefix,
     running,
@@ -84,6 +101,8 @@
     w_sem,
     t_send,
     t_recv,
+    x_send,
+    x_recv,
     f_send,
     f_recv,
     e_send,
@@ -169,11 +188,18 @@
         )
 
     def token_copy(q):
-        other = across if q == 0 else near(q)
-        return remote(tok.at[t], tok.at[t], t_send.at[q], t_recv.at[q], s, other)
-
-    def forward_copy(q):
-        return remote(tok.at[across], tok.at[across], f_send.at[q], f_recv.at[q], s, near(q))
+        return remote(tok.at[t], tok.at[t], t_send.at[q], t_recv.at[q], s, near(q))
+
+    chunks = chunks_of(share)
+    rows_each = share // chunks
+
+    def across_copy(c):
+        some = tok.at[t, pl.ds(c * rows_each, rows_each), :]
+        return remote(some, some, x_send.at[c], x_recv.at[c], s, across)
+
+    def forward_copy(q, c):
+        some = tok.at[across, pl.ds(c * rows_each, rows_each), :]
+        return remote(some, some, f_send.at[q, c], f_recv.at[q, c], s, near(q))
 
     def edge_copy(q):
         return remote(edge_out, edge_in.at[0], e_send.at[q], e_recv.at[0], s + 1, q)
@@ -194,7 +220,9 @@
         for q in range(half):
             middle_copy(q).start()
 
-    for q in range(half):
+    for c in range(chunks):
+        across_copy(c).start()
+    for q in range(1, half):
         token_copy(q).start()
 
     rows_i = lax.broadcasted_iota(jnp.int32, (width, width), 0)
@@ -203,6 +231,7 @@
     incl = cols_i <= rows_i
     eye = jnp.where(cols_i == rows_i, 1.0, 0.0).astype(F32)
     ones = jnp.where(incl, 1.0, 0.0).astype(BF16)
+    incl_two = jnp.concatenate([jnp.where(incl, 1.0, 0.0)] * 2, axis=1) > 0.5
     zeros = jnp.zeros((width, HEAD), F32)
     levels = []
     size = 1
@@ -221,14 +250,14 @@
         scale = lax.rsqrt(jnp.mean(x * x, axis=1, keepdims=True) + norm_floor)
         return (x * scale * ngain).astype(BF16)
 
-    tile = 32
+    tile = 16
     span = half * share
 
-    def norm_block(owner, place):
-        @pl.loop(0, share // tile)
+    def norm_block(owner, place, begin=0, number=share):
+        @pl.loop(0, number // tile)
         def _(i):
-            rows = pl.ds(pl.multiple_of(i * tile, tile), tile)
-            to = pl.ds(pl.multiple_of(place * share + i * tile, tile), tile)
+            rows = pl.ds(pl.multiple_of(begin + i * tile, tile), tile)
+            to = pl.ds(pl.multiple_of(place * share + begin + i * tile, tile), tile)
             normed[to, :] = norm(tok[owner, rows, :].astype(F32))
 
     def project(first, extra):
@@ -243,73 +272,83 @@
             else:
                 proj[j, to, :] = dot1(normed[:span, :], weights[j], NN).astype(BF16)
 
-    def prepare(b):
-        at = pl.ds(pl.multiple_of(b * width, width), width)
-
-        def shifted(j):
-            cur = proj[j, at, :].astype(F32)
-            earlier = jnp.where(first_row, last_row[j, 0:1, :], pltpu.roll(cur, 1, 0))
-            last_row[j] = jnp.broadcast_to(cur[width - 1 :, :], (8, channels))
-            return cur + (earlier - cur) * mix[j : j + 1, :]
-
-        recept, key, value = shifted(0), shifted(1), shifted(2)
-        level = dbase + proj[3, at, :].astype(F32) + drift_ref[b * width]
-        logs = -0.6065306597126334 * jax.nn.sigmoid(level)
-        rate = jax.nn.sigmoid(rbase + proj[4, at, :].astype(F32))
-        total = sum_rows(logs, ones)
-        through = jnp.exp(total)
-        until = jnp.exp(total - logs)
-        inverse = jnp.exp(-total)
-        key_s = key * inverse
-        rec_s = recept * through
-        final = through[width - 1 :, :]
-        rate_inv = rate * inverse
-        every = range(heads)
-        chans = [slice(h * HEAD, (h + 1) * HEAD) for h in every]
-        units = []
-        for ch in chans:
-            key_h = key[:, ch]
-            units.append(key_h * lax.rsqrt(jnp.sum(key_h * key_h, axis=1, keepdims=True) + 1.0))
-        alphas = [-units[h] * until[:, chans[h]] for h in every]
-        betas = [units[h] * rate_inv[:, chans[h]] for h in every]
-        keys = [key_s[:, ch] for ch in chans]
-        recs = [rec_s[:, ch] for ch in chans]
-        vals = [value[:, ch] for ch in chans]
-        fins = [final[:, ch] for ch in chans]
+    def prepare(bs):
+        units, alphas, betas, keys, vals, fins, cross, recs = [], [], [], [], [], [], [], []
+        for b in bs:
+            at = pl.ds(pl.multiple_of(b * width, width), width)
+
+            def shifted(j):
+                cur = proj[j, at, :].astype(F32)
+                earlier = jnp.where(first_row, last_row[j, 0:1, :], pltpu.roll(cur, 1, 0))
+                last_row[j] = jnp.broadcast_to(cur[width - 1 :, :], (8, channels))
+                return cur + (earlier - cur) * mix[j : j + 1, :]
+
+            recept, key, value = shifted(0), shifted(1), shifted(2)
+            level = dbase + proj[3, at, :].astype(F32) + drift_ref[b * width]
+            logs = -0.6065306597126334 * jax.nn.sigmoid(level)
+            rate = jax.nn.sigmoid(rbase + proj[4, at, :].astype(F32))
+            total = sum_rows(logs, ones)
+            through = jnp.exp(total)
+            until = jnp.exp(total - logs)
+            inverse = jnp.exp(-total)
+            key_s = key * inverse
+            rec_s = recept * through
+            final = through[width - 1 :, :]
+            rate_inv = rate * inverse
+            for h in range(heads):
+                ch = slice(h * HEAD, (h + 1) * HEAD)
+                key_h = key[:, ch]
+                unit = key_h * lax.rsqrt(jnp.sum(key_h * key_h, axis=1, keepdims=True) + 1.0)
+                units.append((b, h))
+                alphas.append(-unit * until[:, ch])
+                betas.append(unit * rate_inv[:, ch])
+                keys.append(key_s[:, ch])
+                vals.append(value[:, ch])
+                fins.append(final[:, ch])
+                recs.append(rec_s[:, ch])
+                reads[b, h, :, :HEAD] = rec_s[:, ch]
+        every = range(len(units))
         cross = [
             mm(
-                jnp.concatenate([alphas[h], recs[h]], axis=0),
-                jnp.concatenate([betas[h], keys[h]], axis=0),
+                jnp.concatenate([alphas[u], recs[u]], axis=0),
+                jnp.concatenate([betas[u], keys[u]], axis=0),
                 NT,
             )
-            for h in every
+            for u in every
         ]
+        for u in every:
+            ups[units[u]] = jnp.where(incl_two, cross[u][width:, :], 0.0).astype(BF16)
         low_ab = [jnp.where(strict, c[:width, :width], 0.0) for c in cross]
         low_ak = [jnp.where(strict, c[:width, width:], 0.0) for c in cross]
-        up_b = [jnp.where(incl, c[width:, :width], 0.0) for c in cross]
-        up_k = [jnp.where(incl, c[width:, width:], 0.0) for c in cross]
-        both = [mm(jnp.concatenate([low_ak[h], up_k[h]], axis=0), vals[h]) for h in every]
+        both = [mm(low_ak[u], vals[u]) for u in every]
         inv = [eye + jnp.where(levels[0], low, 0.0) for low in low_ab]
         for mask in levels[1:]:
-            right = [mm(jnp.where(mask, low_ab[h], 0.0), inv[h]) for h in every]
-            inv = [inv[h] + mm(inv[h], right[h]) for h in every]
-        solved = [
-            mm(inv[h], jnp.concatenate([alphas[h], both[h][:width]], axis=1)) for h in every
-        ]
-        for h in every:
-            reads[b, h] = jnp.concatenate([recs[h], both[h][width:]], axis=1) + mm(
-                up_b[h], solved[h]
+            short = [i.astype(BF16) for i in inv]
+            right = [mm1(jnp.where(mask, low_ab[u], 0.0), short[u]) for u in every]
+            inv = [inv[u] + mm1(short[u], right[u]) for u in every]
+        solved = [mm(inv[u], jnp.concatenate([alphas[u], both[u]], axis=1)) for u in every]
+        for u in every:
+            ends = jnp.concatenate([betas[u] * fins[u], keys[u] * fins[u]], axis=0)
+            column = jnp.concatenate(
+                [solved[u], jnp.concatenate([zeros, vals[u]], axis=1)], axis=0
             )
-        for h in every:
-            ends = jnp.concatenate([betas[h] * fins[h], keys[h] * fins[h]], axis=0)
-            piece = mm(
-                ends,
-                jnp.concatenate(
-                    [solved[h], jnp.concatenate([zeros, vals[h]], axis=1)], axis=0
-                ),
-                TN,
+            stack[units[u]] = column.astype(BF16)
+            pieces[units[u]] = mm(ends, column, TN) + jnp.concatenate(
+                [eye * fins[u], zeros], axis=1
             )
-            pieces[b, h] = piece + jnp.concatenate([eye * fins[h], zeros], axis=1)
+
+    def centered(x):
+        return x - jnp.mean(x, axis=1, keepdims=True)
+
+    def defer(b):
+        at = pl.ds(pl.multiple_of(b * width, width), width)
+        for h in range(heads):
+            made = dot1(ups[b, h], stack[b, h], NN)
+            read = reads[b, h, :, :HEAD] + made[:, :HEAD]
+            both = mm(read, prefix[b, h])
+            fixed = centered(both[:, HEAD:] + made[:, HEAD:])
+            final_reads[h, at, :] = jnp.concatenate([both[:, :HEAD], fixed], axis=1)
+        gates[at, :] = jax.nn.sigmoid(proj[5, at, :].astype(F32)) * gain
 
     def open_half(which):
         for j in range(3):
@@ -349,28 +388,30 @@
     project(base, True)
     open_half(upper)
 
-    @pl.loop(0, blocks // 2)
-    def _(i):
-        prepare(upper * (blocks // 2) + i)
-
-        @pl.when(i == 0)
-        def _():
-            token_copy(0).wait_recv()
-            for q in range(1, half):
-                forward_copy(q).start()
+    group = max(g for g in (1, 2, 3) if (blocks // 2) % g == 0)
+
+    def prepare_half(first):
+        @pl.loop(0, blocks // 2 // group)
+        def _(i):
+            prepare([first + i * group + g for g in range(group)])
+
+    prepare_half(upper * (blocks // 2))
 
     lower = 1 - upper
-    norm_block(across, across - lower * half)
+    for c in range(chunks):
+        across_copy(c).wait_recv()
+        for q in range(1, half):
+            forward_copy(q, c).start()
+        norm_block(across, across - lower * half, c * rows_each, rows_each)
     for q in range(1, half):
-        forward_copy(q).wait_recv()
         far = lower * half + near(half - q) - base
-        norm_block(far, far - lower * half)
+        for c in range(chunks):
+            forward_copy(q, c).wait_recv()
+            norm_block(far, far - lower * half, c * rows_each, rows_each)
     project(lower * half, False)
     open_half(lower)
 
-    @pl.loop(0, blocks // 2)
-    def _(i):
-        prepare(lower * (blocks // 2) + i)
+    prepare_half(lower * (blocks // 2))
 
     def joined(later, earlier):
         return mm(later[:, :HEAD], earlier) + jnp.concatenate([zeros, later[:, HEAD:]], axis=1)
@@ -389,7 +430,9 @@
         own = running[h]
         start = jnp.concatenate([zeros, init_ref[h].T], axis=1)
         window[h] = jnp.where(at_start, start, jnp.concatenate([eye, zeros], axis=1))
-        g_buf[0, h] = jnp.where(at_start, joined(own, start), own)
+        whole = jnp.where(at_start, joined(own, start), own)
+        running[h] = whole
+        g_buf[0, h] = whole.astype(BF16)
 
     def hop(k):
         return remote(g_buf.at[k], r_buf.at[k], g_send.at[k], g_recv.at[k], s + steps[k], t)
@@ -399,40 +442,49 @@
         @pl.when(s + d < n)
         def _():
             hop(k).start()
+
+        @pl.loop(k * blocks // len(steps), (k + 1) * blocks // len(steps))
+        def _(b):
+            defer(b)
 
         @pl.when(s - d >= 0)
         def _():
             hop(k).wait_recv()
             for h in range(heads):
-                window[h] = joined(window[h], r_buf[k, h])
+                now = window[h]
+                window[h] = mm2(now[:, :HEAD], r_buf[k, h]) + jnp.concatenate(
+                    [zeros, now[:, HEAD:]], axis=1
+                )
 
         if k + 1 < len(steps):
             for h in range(heads):
-                g_buf[k + 1, h] = jnp.where(at_start, g_buf[k, h], joined(running[h], window[h]))
-
-    @pl.loop(0, blocks)
-    def _(b):
-        at = pl.ds(pl.multiple_of(b * width, width), width)
-        gate = jax.nn.sigmoid(proj[5, at, :].astype(F32))
+                whole = jnp.where(at_start, running[h], joined(running[h], window[h]))
+                g_buf[k + 1, h] = whole.astype(BF16)
+
+    entry = [split(centered(window[h][:, HEAD:])) for h in range(heads)]
+
+    def finish(dest):
+        at = pl.ds(pl.multiple_of(dest * share, share), share)
         parts = []
         for h in range(heads):
-            now = prefix[b, h]
-            state = mm(now[:, :HEAD], window[h][:, HEAD:]) + now[:, HEAD:]
-            read = reads[b, h]
-            mixed = mm(read[:, :HEAD], state) + read[:, HEAD:]
-            center = mixed - jnp.mean(mixed, axis=1, keepdims=True)
+            read = final_reads[h, at, :]
+            high, low = split(read[:, :HEAD])
+            center = dot1(high, entry[h][0], NN) + (
+                dot1(high, entry[h][1], NN) + dot1(low, entry[h][0], NN)
+            )
+            center = center + read[:, HEAD:]
             spread = jnp.mean(center * center, axis=1, keepdims=True)
             parts.append(center * lax.rsqrt(spread + group_floor))
-        gated[at, :] = (jnp.concatenate(parts, axis=1) * gain * gate).astype(BF16)
+        return (jnp.concatenate(parts, axis=1) * gates[at, :]).astype(BF16)
 
     def part(q):
         dest = lax.rem(t + q, m)
-        rows = pl.ds(pl.multiple_of(dest * share, share), share)
-        return remote(gated.at[rows, :], act.at[t], a_send.at[q], a_recv.at[q], s, dest)
+        return remote(gated.at[q - 1], act.at[t], a_send.at[q], a_recv.at[q], s, dest)
 
     for q in range(1, m):
+        gated[q - 1] = finish(lax.rem(t + q, m))
         part(q).start()
-    act[t] = gated[pl.ds(pl.multiple_of(t * share, share), share), :]
+    act[t] = finish(t)
     out_load.wait()
     for q in range(1, m):
         part(q).wait_recv()
@@ -443,10 +495,12 @@
         out_ref[:, c : c + out_tile] = dot1(rows, wout[:, c : c + out_tile], NN).astype(BF16)
     for q in range(1, m):
         part(q).wait_send()
-    for q in range(half):
+    for c in range(chunks):
+        across_copy(c).wait_send()
+    for q in range(1, half):
         token_copy(q).wait_send()
-    for q in range(1, half):
-        forward_copy(q).wait_send()
+        for c in range(chunks):
+            forward_copy(q, c).wait_send()
 
     @pl.when(has_next)
     def _():
@@ -512,21 +566,27 @@
             pltpu.VMEM((3, 16, width), F32),
             pltpu.VMEM((3, 8, width), F32),
             pltpu.VMEM((blocks, heads, BLOCK, 2 * HEAD), F32),
+            pltpu.VMEM((blocks, heads, BLOCK, 2 * HEAD), BF16),
+            pltpu.VMEM((blocks, heads, 2 * BLOCK, 2 * HEAD), BF16),
+            pltpu.VMEM((heads, seq, 2 * HEAD), F32),
+            pltpu.VMEM((seq, width), F32),
             pltpu.VMEM((blocks, heads, HEAD, 2 * HEAD), F32),
             pltpu.VMEM((blocks, heads, HEAD, 2 * HEAD), F32),
             pltpu.VMEM((heads, HEAD, 2 * HEAD), F32),
             pltpu.VMEM((heads, HEAD, 2 * HEAD), F32),
-            pltpu.VMEM((hops, heads, HEAD, 2 * HEAD), F32),
-            pltpu.VMEM((hops, heads, HEAD, 2 * HEAD), F32),
-            pltpu.VMEM((seq, width), BF16),
+            pltpu.VMEM((hops, heads, HEAD, 2 * HEAD), BF16),
+            pltpu.VMEM((hops, heads, HEAD, 2 * HEAD), BF16),
+            pltpu.VMEM((m - 1, share, width), BF16),
             pltpu.VMEM((m, share, width), BF16),
             pltpu.VMEM(w_out.shape, BF16),
             dma,
             dma((7,)),
             dma((m,)),
             dma((m,)),
-            dma((m,)),
-            dma((m,)),
+            dma((chunks_of(share),)),
+            dma((chunks_of(share),)),
+            dma((m, chunks_of(share))),
+            dma((m, chunks_of(share))),
             dma((m,)),
             dma((2,)),
             dma((hops,)),

time: 56.8 us -> 41.8 us (0.74)
  the two profiles are of different devices: /device:TPU:27 before, /device:TPU:19 now
where the time goes in v3:
time: 41.8 us; the launch traced here: 41.6 us
  Pallas kernels  39.9 us (95%)
  local copies, waits for them, and re-layouts  1.77 us (4%)
    pallas_call x1, Pallas kernels, per_device(): pl.pallas_call(functools.partial(layer_kernel, n, m, heads, blocks), out_...  39.9 us
    unnamed x1, local copies, waits for them, and re-layouts  1.77 us

profile of v3, /device:TPU:19, one launch (start us, length us, event | category | flops | bytes accessed | tf_op | source)
XLA Modules:
  0.0 41.6 jit_solution(4834683034372972438)
XLA Ops:
  0.0 39.9 %layer_kernel.1 = bf16[96,2048]{1,0:T(8,128)(2,1)} custom-call(f32[384]{0:T(512)} %drift_ref.1, bf16[96,2048]{1,0:T(8,128)(2,1)} %tok_ref.1, f32[2048]{0:T(1024)} %ngain_ref.1, bf16[2048,256]{1,0:T(8,128)(2,1)} %wr_ref.1, bf16[2048,256]{1,0:T(8,128)(2,1)} %wk_ref.1, bf16[2048,256]{1,0:T(8,128)(2,1)} %wv_ref.1, bf16[2048,256]{1,0:T(8,128)(2,1)} %wd_ref.1, ...), custom_call_target="tpu_custom_call" | custom-call | tf_op jit(solution)/shard_map/layer_kernel/pallas_call | solution.py:551
  39.9 1.8 %copy.17 = bf16[96,2048]{1,0:T(8,128)(2,1)} copy(bf16[96,2048]{1,0:T(8,128)(2,1)} %layer_kernel.1) | data formatting | bytes 786432

commit v4 on v3

--- a/solution.py
+++ b/solution.py
@@ -94,6 +94,8 @@
     window,
     g_buf,
     r_buf,
+    c_out,
+    c_in,
     gated,
     act,
     wout,
@@ -138,7 +140,6 @@
     for load in loads:
         load.start()
     out_load = pltpu.make_async_copy(wout_ref, wout, w_sem.at[len(sources)])
-    out_load.start()
 
     barrier = pltpu.get_barrier_semaphore()
     count = m - 1
@@ -386,6 +387,7 @@
         jnp.concatenate(joined_rows + [jnp.zeros((14, depth), F32)], axis=0)
     )
     project(base, True)
+    out_load.start()
     open_half(upper)
 
     group = max(g for g in (1, 2, 3) if (blocks // 2) % g == 0)
@@ -432,10 +434,23 @@
         window[h] = jnp.where(at_start, start, jnp.concatenate([eye, zeros], axis=1))
         whole = jnp.where(at_start, joined(own, start), own)
         running[h] = whole
-        g_buf[0, h] = whole.astype(BF16)
+
+    final_hop = len(steps) - 1
+
+    def offer(k, wholes):
+        if k < final_hop:
+            for h in range(heads):
+                g_buf[k, h] = wholes[h].astype(BF16)
+        else:
+            for p in range(heads // 2):
+                pair = [wholes[2 * p][:, HEAD:], wholes[2 * p + 1][:, HEAD:]]
+                c_out[p] = jnp.concatenate(pair, axis=1).astype(BF16)
+
+    offer(0, [running[h] for h in range(heads)])
 
     def hop(k):
-        return remote(g_buf.at[k], r_buf.at[k], g_send.at[k], g_recv.at[k], s + steps[k], t)
+        src, dst = (g_buf.at[k], r_buf.at[k]) if k < final_hop else (c_out, c_in)
+        return remote(src, dst, g_send.at[k], g_recv.at[k], s + steps[k], t)
 
     for k, d in enumerate(steps):
 
@@ -452,14 +467,23 @@
             hop(k).wait_recv()
             for h in range(heads):
                 now = window[h]
-                window[h] = mm2(now[:, :HEAD], r_buf[k, h]) + jnp.concatenate(
-                    [zeros, now[:, HEAD:]], axis=1
-                )
+                if k < final_hop:
+                    window[h] = mm2(now[:, :HEAD], r_buf[k, h]) + jnp.concatenate(
+                        [zeros, now[:, HEAD:]], axis=1
+                    )
+                else:
+                    lane = (h % 2) * HEAD
+                    got = mm2(now[:, :HEAD], c_in[h // 2])[:, lane : lane + HEAD]
+                    window[h] = jnp.concatenate([zeros, got + now[:, HEAD:]], axis=1)
 
         if k + 1 < len(steps):
-            for h in range(heads):
-                whole = jnp.where(at_start, running[h], joined(running[h], window[h]))
-                g_buf[k + 1, h] = whole.astype(BF16)
+            offer(
+                k + 1,
+                [
+                    jnp.where(at_start, running[h], joined(running[h], window[h]))
+                    for h in range(heads)
+                ],
+            )
 
     entry = [split(centered(window[h][:, HEAD:])) for h in range(heads)]
 
@@ -576,6 +600,8 @@
             pltpu.VMEM((heads, HEAD, 2 * HEAD), F32),
             pltpu.VMEM((hops, heads, HEAD, 2 * HEAD), BF16),
             pltpu.VMEM((hops, heads, HEAD, 2 * HEAD), BF16),
+            pltpu.VMEM((heads // 2, HEAD, 2 * HEAD), BF16),
+            pltpu.VMEM((heads // 2, HEAD, 2 * HEAD), BF16),
             pltpu.VMEM((m - 1, share, width), BF16),
             pltpu.VMEM((m, share, width), BF16),
             pltpu.VMEM(w_out.shape, BF16),

time: 41.8 us -> 39.8 us (0.952)
  the two profiles are of different devices: /device:TPU:19 before, /device:TPU:27 now
where the time goes in v4:
time: 39.8 us; the launch traced here: 39.1 us
  Pallas kernels  37.3 us (94%)
  local copies, waits for them, and re-layouts  1.77 us (4%)
    pallas_call x1, Pallas kernels, per_device(): pl.pallas_call(functools.partial(layer_kernel, n, m, heads, blocks), out_...  37.3 us
    unnamed x1, local copies, waits for them, and re-layouts  1.77 us

profile of v4, /device:TPU:27, one launch (start us, length us, event | category | flops | bytes accessed | tf_op | source)
XLA Modules:
  0.0 39.1 jit_solution(9315860541469874703)
XLA Ops:
  0.0 37.3 %layer_kernel.1 = bf16[96,2048]{1,0:T(8,128)(2,1)} custom-call(f32[384]{0:T(512)} %drift_ref.1, bf16[96,2048]{1,0:T(8,128)(2,1)} %tok_ref.1, f32[2048]{0:T(1024)} %ngain_ref.1, bf16[2048,256]{1,0:T(8,128)(2,1)} %wr_ref.1, bf16[2048,256]{1,0:T(8,128)(2,1)} %wk_ref.1, bf16[2048,256]{1,0:T(8,128)(2,1)} %wv_ref.1, bf16[2048,256]{1,0:T(8,128)(2,1)} %wd_ref.1, ...), custom_call_target="tpu_custom_call" | custom-call | tf_op jit(solution)/shard_map/layer_kernel/pallas_call | solution.py:575
  37.3 1.8 %copy.17 = bf16[96,2048]{1,0:T(8,128)(2,1)} copy(bf16[96,2048]{1,0:T(8,128)(2,1)} %layer_kernel.1) | data formatting | bytes 786432

commit v5 on v4

--- a/solution.py
+++ b/solution.py
@@ -73,7 +73,6 @@
     rbase_ref,
     gain_ref,
     init_ref,
-    wout_ref,
     out_ref,
     tok,
     edge_out,
@@ -98,7 +97,6 @@
     c_in,
     gated,
     act,
-    wout,
     own_sem,
     w_sem,
     t_send,
@@ -139,7 +137,6 @@
     ]
     for load in loads:
         load.start()
-    out_load = pltpu.make_async_copy(wout_ref, wout, w_sem.at[len(sources)])
 
     barrier = pltpu.get_barrier_semaphore()
     count = m - 1
@@ -387,7 +384,6 @@
         jnp.concatenate(joined_rows + [jnp.zeros((14, depth), F32)], axis=0)
     )
     project(base, True)
-    out_load.start()
     open_half(upper)
 
     group = max(g for g in (1, 2, 3) if (blocks // 2) % g == 0)
@@ -509,14 +505,10 @@
         gated[q - 1] = finish(lax.rem(t + q, m))
         part(q).start()
     act[t] = finish(t)
-    out_load.wait()
     for q in range(1, m):
         part(q).wait_recv()
-    rows = jnp.concatenate([act[q] for q in range(m)], axis=1)
-    columns = out_ref.shape[1]
-    out_tile = min(512, columns)
-    for c in range(0, columns, out_tile):
-        out_ref[:, c : c + out_tile] = dot1(rows, wout[:, c : c + out_tile], NN).astype(BF16)
+    for q in range(m):
+        out_ref[:, q * channels : (q + 1) * channels] = act[q]
     for q in range(1, m):
         part(q).wait_send()
     for c in range(chunks):
@@ -570,15 +562,14 @@
     hops = max(1, (n - 1).bit_length())
     lanes = 128
     vmem = pl.BlockSpec(memory_space=pltpu.VMEM)
-    anywhere = pl.BlockSpec(memory_space=pl.ANY)
+    anywhere = pl.BlockSpec(memory_space=pltpu.MemorySpace.HBM)
     dma = pltpu.SemaphoreType.DMA
-    return pl.pallas_call(
+    rows = pl.pallas_call(
         functools.partial(layer_kernel, n, m, heads, blocks),
-        out_shape=jax.ShapeDtypeStruct((share, w_out.shape[1]), BF16),
+        out_shape=jax.ShapeDtypeStruct((share, m * width), BF16),
         in_specs=[pl.BlockSpec(memory_space=pltpu.SMEM), anywhere, vmem]
         + [anywhere] * 6
-        + [vmem] * 5
-        + [anywhere],
+        + [vmem] * 5,
         out_specs=vmem,
         scratch_shapes=[
             pltpu.VMEM((m, share, depth), BF16),
@@ -604,9 +595,8 @@
             pltpu.VMEM((heads // 2, HEAD, 2 * HEAD), BF16),
             pltpu.VMEM((m - 1, share, width), BF16),
             pltpu.VMEM((m, share, width), BF16),
-            pltpu.VMEM(w_out.shape, BF16),
             dma,
-            dma((7,)),
+            dma((6,)),
             dma((m,)),
             dma((m,)),
             dma((chunks_of(share),)),
@@ -621,7 +611,7 @@
             dma((m,)),
         ],
         compiler_params=pltpu.CompilerParams(
-            collective_id=1, has_side_effects=True, vmem_limit_bytes=60 * 1024 * 1024
+            collective_id=1, has_side_effects=True, vmem_limit_bytes=40 * 1024 * 1024
         ),
         name="layer_kernel",
     )(
@@ -639,8 +629,8 @@
         rate_base,
         group_gain,
         initial_state,
-        w_out,
     )
+    return jnp.dot(rows, w_out, preferred_element_type=F32).astype(BF16)
 
 
 def solution(mesh):

time: 39.8 us -> 51.5 us (1.29)
  local copies, waits for them, and re-layouts: 1.77 us -> 13.3 us
  matrix products: 0 us -> 1.55 us
  Pallas kernels: 37.3 us -> 35.8 us
    unnamed x1 -> x30, local copies, waits for them, and re-layouts: 1.77 us -> 13.3 us
    dot_general x0 -> x1, matrix products: none -> 1.55 us  [per_device(): return jnp.dot(rows, w_out, preferred_element_type=F32).astype(BF16)]
    pallas_call x1, Pallas kernels: 37.3 us -> 35.8 us  [per_device(): pl.pallas_call(functools.partial(layer_kernel, n, m, heads, blocks), out_...]
where the time goes in v5:
time: 51.5 us; the launch traced here: 50.8 us
  Pallas kernels  35.8 us (70%)
  local copies, waits for them, and re-layouts  13.3 us (26%)
  matrix products  1.55 us (3%)
    pallas_call x1, Pallas kernels, per_device(): pl.pallas_call(functools.partial(layer_kernel, n, m, heads, blocks), out_...  35.8 us
    unnamed x30, local copies, waits for them, and re-layouts  13.3 us
    dot_general x1, matrix products, per_device(): return jnp.dot(rows, w_out, preferred_element_type=F32).astype(BF16)  1.55 us

profile of v5, /device:TPU:27, one launch (start us, length us, event | category | flops | bytes accessed | tf_op | source)
XLA Modules:
  0.0 50.8 jit_solution(7266445078913541950)
XLA Ops:
  0.0 0.0 copy-start
  0.0 1.2 %copy-done = bf16[2048,256]{1,0:T(8,128)(2,1)S(1)} copy-done((bf16[2048,256]{1,0:T(8,128)(2,1)S(1)}, bf16[2048,256]{1,0:T(8,128)(2,1)}, u32[]{:S(2)}) %copy-start) | copy-done | bytes 1048600
  1.2 0.0 copy-start.1
  1.2 1.2 %copy-done.1 = bf16[2048,256]{1,0:T(8,128)(2,1)S(1)} copy-done((bf16[2048,256]{1,0:T(8,128)(2,1)S(1)}, bf16[2048,256]{1,0:T(8,128)(2,1)}, u32[]{:S(2)}) %copy-start.1) | copy-done | bytes 1048600
  2.5 0.0 copy-start.2
  2.5 1.2 %copy-done.2 = bf16[2048,256]{1,0:T(8,128)(2,1)S(1)} copy-done((bf16[2048,256]{1,0:T(8,128)(2,1)S(1)}, bf16[2048,256]{1,0:T(8,128)(2,1)}, u32[]{:S(2)}) %copy-start.2) | copy-done | bytes 1048600
  3.7 0.0 copy-start.3
  3.7 1.2 %copy-done.3 = bf16[2048,256]{1,0:T(8,128)(2,1)S(1)} copy-done((bf16[2048,256]{1,0:T(8,128)(2,1)S(1)}, bf16[2048,256]{1,0:T(8,128)(2,1)}, u32[]{:S(2)}) %copy-start.3) | copy-done | bytes 1048600
  4.9 0.0 copy-start.4
  4.9 1.2 %copy-done.4 = bf16[2048,256]{1,0:T(8,128)(2,1)S(1)} copy-done((bf16[2048,256]{1,0:T(8,128)(2,1)S(1)}, bf16[2048,256]{1,0:T(8,128)(2,1)}, u32[]{:S(2)}) %copy-start.4) | copy-done | bytes 1048600
  6.1 0.0 copy-start.5
  6.1 1.2 %copy-done.5 = bf16[2048,256]{1,0:T(8,128)(2,1)S(1)} copy-done((bf16[2048,256]{1,0:T(8,128)(2,1)S(1)}, bf16[2048,256]{1,0:T(8,128)(2,1)}, u32[]{:S(2)}) %copy-start.5) | copy-done | bytes 1048600
  7.4 0.0 copy-start.6
  7.4 1.0 %copy-done.6 = bf16[96,2048]{1,0:T(8,128)(2,1)S(1)} copy-done((bf16[96,2048]{1,0:T(8,128)(2,1)S(1)}, bf16[96,2048]{1,0:T(8,128)(2,1)}, u32[]{:S(2)}) %copy-start.6) | copy-done | bytes 393240
  8.3 0.0 copy-start.7
  8.4 0.9 %copy-done.7 = f32[4,64,64]{2,1,0:T(8,128)S(1)} copy-done((f32[4,64,64]{2,1,0:T(8,128)S(1)}, f32[4,64,64]{2,1,0:T(8,128)}, u32[]{:S(2)}) %copy-start.7) | copy-done | bytes 65560
  9.3 0.0 copy-start.8
  9.3 0.7 %copy-done.8 = f32[2048]{0:T(1024)S(1)} copy-done((f32[2048]{0:T(1024)S(1)}, f32[2048]{0:T(1024)}, u32[]{:S(2)}) %copy-start.8) | copy-done | bytes 8216
  10.0 0.0 copy-start.9
  10.0 0.7 %copy-done.9 = f32[3,256]{1,0:T(4,128)S(1)} copy-done((f32[3,256]{1,0:T(4,128)S(1)}, f32[3,256]{1,0:T(4,128)}, u32[]{:S(2)}) %copy-start.9) | copy-done | bytes 3096
  10.6 0.0 copy-start.10
  10.6 0.7 %copy-done.10 = f32[384]{0:T(512)S(1)} copy-done((f32[384]{0:T(512)S(1)}, f32[384]{0:T(512)}, u32[]{:S(2)}) %copy-start.10) | copy-done | bytes 1560
  11.3 0.0 copy-start.11
  11.3 0.7 %copy-done.11 = f32[256]{0:T(256)S(1)} copy-done((f32[256]{0:T(256)S(1)}, f32[256]{0:T(256)}, u32[]{:S(2)}) %copy-start.11) | copy-done | bytes 1048
  12.0 0.0 copy-start.12
  12.0 0.7 %copy-done.12 = f32[256]{0:T(256)S(1)} copy-done((f32[256]{0:T(256)S(1)}, f32[256]{0:T(256)}, u32[]{:S(2)}) %copy-start.12) | copy-done | bytes 1048
  12.7 0.0 copy-start.13
  12.7 0.7 %copy-done.13 = f32[256]{0:T(256)S(1)} copy-done((f32[256]{0:T(256)S(1)}, f32[256]{0:T(256)}, u32[]{:S(2)}) %copy-start.13) | copy-done | bytes 1048
  13.4 0.0 copy-start.14
  13.4 35.8 %layer_kernel.1 = bf16[96,1024]{1,0:T(8,128)(2,1)S(1)} custom-call(f32[384]{0:T(512)S(1)} %copy-done.10, bf16[96,2048]{1,0:T(8,128)(2,1)S(1)} %copy-done.6, f32[2048]{0:T(1024)S(1)} %copy-done.8, bf16[2048,256]{1,0:T(8,128)(2,1)S(1)} %copy-done, bf16[2048,256]{1,0:T(8,128)(2,1)S(1)} %copy-done.1, bf16[2048,256]{1,0:T(8,128)(2,1)S(1)} %copy-done.2, ...), custom_call_target="tpu_custom_call" | custom-call | tf_op jit(solution)/shard_map/layer_kernel/pallas_call | solution.py:567
  49.2 0.0 copy-done.14
  49.2 1.6 %convolution_convert_fusion = bf16[96,2048]{1,0:T(8,128)(2,1)} fusion(bf16[96,1024]{1,0:T(8,128)(2,1)S(1)} %layer_kernel.1, bf16[1024,2048]{1,0:T(8,128)(2,1)S(1)} %copy-done.14), kind=kOutput, calls=%fused_computation | convolution fusion | flops 402849792 | bytes 4784128 | tf_op jit(solution)/shard_map/dot_general | solution.py:633
Async XLA Ops:
  0.0 1.2 %copy-start = (bf16[2048,256]{1,0:T(8,128)(2,1)S(1)}, bf16[2048,256]{1,0:T(8,128)(2,1)}, u32[]{:S(2)}) copy-start(bf16[2048,256]{1,0:T(8,128)(2,1)} %wr_ref.1) | copy-start | bytes 3145732
  1.2 1.2 %copy-start.1 = (bf16[2048,256]{1,0:T(8,128)(2,1)S(1)}, bf16[2048,256]{1,0:T(8,128)(2,1)}, u32[]{:S(2)}) copy-start(bf16[2048,256]{1,0:T(8,128)(2,1)} %wk_ref.1) | copy-start | bytes 3145732
  2.5 1.2 %copy-start.2 = (bf16[2048,256]{1,0:T(8,128)(2,1)S(1)}, bf16[2048,256]{1,0:T(8,128)(2,1)}, u32[]{:S(2)}) copy-start(bf16[2048,256]{1,0:T(8,128)(2,1)} %wv_ref.1) | copy-start | bytes 3145732
  3.7 1.2 %copy-start.3 = (bf16[2048,256]{1,0:T(8,128)(2,1)S(1)}, bf16[2048,256]{1,0:T(8,128)(2,1)}, u32[]{:S(2)}) copy-start(bf16[2048,256]{1,0:T(8,128)(2,1)} %wd_ref.1) | copy-start | bytes 3145732
  4.9 1.2 %copy-start.4 = (bf16[2048,256]{1,0:T(8,128)(2,1)S(1)}, bf16[2048,256]{1,0:T(8,128)(2,1)}, u32[]{:S(2)}) copy-start(bf16[2048,256]{1,0:T(8,128)(2,1)} %wa_ref.1) | copy-start | bytes 3145732
  6.1 1.2 %copy-start.5 = (bf16[2048,256]{1,0:T(8,128)(2,1)S(1)}, bf16[2048,256]{1,0:T(8,128)(2,1)}, u32[]{:S(2)}) copy-start(bf16[2048,256]{1,0:T(8,128)(2,1)} %wg_ref.1) | copy-start | bytes 3145732
  7.4 1.0 %copy-start.6 = (bf16[96,2048]{1,0:T(8,128)(2,1)S(1)}, bf16[96,2048]{1,0:T(8,128)(2,1)}, u32[]{:S(2)}) copy-start(bf16[96,2048]{1,0:T(8,128)(2,1)} %tok_ref.1) | copy-start | bytes 1179652
  8.3 0.9 %copy-start.7 = (f32[4,64,64]{2,1,0:T(8,128)S(1)}, f32[4,64,64]{2,1,0:T(8,128)}, u32[]{:S(2)}) copy-start(f32[4,64,64]{2,1,0:T(8,128)} %init_ref.1) | copy-start | bytes 196612
  9.3 0.7 %copy-start.8 = (f32[2048]{0:T(1024)S(1)}, f32[2048]{0:T(1024)}, u32[]{:S(2)}) copy-start(f32[2048]{0:T(1024)} %ngain_ref.1) | copy-start | bytes 24580
  10.0 0.7 %copy-start.9 = (f32[3,256]{1,0:T(4,128)S(1)}, f32[3,256]{1,0:T(4,128)}, u32[]{:S(2)}) copy-start(f32[3,256]{1,0:T(4,128)} %mix_ref.1) | copy-start | bytes 9220
  10.6 0.7 %copy-start.10 = (f32[384]{0:T(512)S(1)}, f32[384]{0:T(512)}, u32[]{:S(2)}) copy-start(f32[384]{0:T(512)} %drift_ref.1) | copy-start | bytes 4612
  11.3 0.7 %copy-start.11 = (f32[256]{0:T(256)S(1)}, f32[256]{0:T(256)}, u32[]{:S(2)}) copy-start(f32[256]{0:T(256)} %dbase_ref.1) | copy-start | bytes 3076
  12.0 0.7 %copy-start.12 = (f32[256]{0:T(256)S(1)}, f32[256]{0:T(256)}, u32[]{:S(2)}) copy-start(f32[256]{0:T(256)} %rbase_ref.1) | copy-start | bytes 3076
  12.7 0.7 %copy-start.13 = (f32[256]{0:T(256)S(1)}, f32[256]{0:T(256)}, u32[]{:S(2)}) copy-start(f32[256]{0:T(256)} %gain_ref.1) | copy-start | bytes 3076
  13.4 35.9 %copy-start.14 = (bf16[1024,2048]{1,0:T(8,128)(2,1)S(1)}, bf16[1024,2048]{1,0:T(8,128)(2,1)}, u32[]{:S(2)}) copy-start(bf16[1024,2048]{1,0:T(8,128)(2,1)} %param.29) | copy-start | bytes 12582916
